TPU v7x, 128 devices: a whole 4x4x4 slice. The times are simulated.
128 devices in a mesh: sp: 16 (over z, x), dp: 8 (over y, core).
Axes of the slice: x: 4, y: 4, z: 4, core: 2. Of those that a mesh axis runs over, the one named last changes fastest.
Arguments:
- queries: bfloat16 [8, 2048, 2048], P('dp', 'sp'), may hold values from -6 to 6
- forget_pre: bfloat16 [8, 2048, 2048], P('dp', 'sp'), may hold values from -5.5 to 5.5
- values: bfloat16 [8, 2048, 2048], P('dp', 'sp'), may hold values from -6 to 6
- out_gate: bfloat16 [8, 2048, 2048], P('dp', 'sp'), may hold values from -6 to 6
- lower_bound: float32 [2048], P('sp'), may hold values from 0.9 to 1, as said below
- head_gain: float32 [128], replicated, may hold values from 0.1 to 1.9
- residual: bfloat16 [8, 2048, 4096], P('dp', 'sp'), may hold values from -6 to 6
- out_weight: bfloat16 [2048, 4096], P(None, 'dp'), may hold values from -0.125 to 0.125
- ffn_gain: float32 [4096], replicated, may hold values from 0.1 to 1.9
- routing: int32 [8, 2048, 4], P('dp', 'sp'), may hold values from 0 to 127, all different within a row; in each aligned block of 128 rows (0 to 127, 128 to 255, ..., all dimensions but the last counted through in order) at most 5 rows name the same one
- route_weight: float32 [8, 2048, 4], P('dp', 'sp'), may hold values from 0.1 to 1
- expert_gate: bfloat16 [128, 4096, 512], P(('sp', 'dp')), may hold values from -0.09375 to 0.09375
- expert_up: bfloat16 [128, 4096, 512], P(('sp', 'dp')), may hold values from -0.09375 to 0.09375
- expert_down: bfloat16 [128, 512, 4096], P(('sp', 'dp')), may hold values from -0.25 to 0.25
Outputs:
- layer_out: bfloat16 [8, 2048, 4096], P('dp', 'sp')
Inputs may be any that keep to these rules, and one draw needn't show every extreme that they name: `routing`: within the rows of one device no expert is named more than 5 times, and in some devices one is named exactly 5 times; the 4 experts of a row differ. `lower_bound`: every entry is below 1.
All inputs are finite; a program needn't handle non-finite values.
Results may differ from a plain program's by a relative error of at most 0.0073.
Values may be sent and summed in bfloat16 or wider, within the bound.
No kernel may reach another device: no remote copies, remote signals or barrier semaphores. Data moves between devices by JAX's collectives and lax.ppermute only.
A program may use at most 128 MiB of HBM per device.

v0:
```python
import jax
import jax.numpy as jnp
from jax import lax
from jax.sharding import PartitionSpec as P

BLOCK = 128


PRECISE = lax.Precision.HIGHEST
NORM_EPS = 1e-06


def side_by_side(arrays, axis, split_dim, concat_dim, along):
    ends, at = ([], 0)
    for a in arrays[:-1]:
        at += a.shape[along]
        ends.append(at)
    both = jnp.concatenate(arrays, axis=along)
    return tuple(
        jnp.split(
            lax.all_to_all(both, axis, split_axis=split_dim, concat_axis=concat_dim, tiled=True),
            ends,
            axis=along,
        )
    )


def split_up(shard, dim, devices):
    before, after = (shard.shape[:dim], shard.shape[dim + 1 :])
    return jnp.moveaxis(shard.reshape(*before, devices, -1, *after), dim, 0)


def piece_ends(length, count):
    unit = 8 if length >= 8 * count else 1
    return [length // unit * k // count * unit for k in range(1, count)]


def in_order(parts, dim):
    lengths = list(parts.shape[1:])
    lengths[dim] *= parts.shape[0]
    return jnp.moveaxis(parts, 0, dim).reshape(lengths)


def cut_exchange(shard, axis, pieces, split_dim, concat_dim):
    parts = split_up(shard, split_dim, lax.axis_size(axis))
    split_at = max(range(1, max(2, parts.ndim - 1)), key=lambda d: parts.shape[d])
    done = []
    for piece in jnp.split(parts, piece_ends(parts.shape[split_at], pieces), axis=split_at):
        if piece.size:
            done.append(lax.all_to_all(piece, axis, split_axis=0, concat_axis=0, tiled=True))
    return in_order(jnp.concatenate(done, axis=split_at), concat_dim)


def forget_terms(forget_pre, lower_bound):
    leak_rate = (1.0 - lower_bound) * jax.nn.sigmoid(-forget_pre.astype(jnp.float32))
    return (jnp.log1p(-leak_rate), leak_rate)


def link_states(earlier, later):
    return (earlier[0] * later[0], later[0][..., None] * earlier[1] + later[1])


def recurrence(query_f, log_keep, key_f, value_f):
    log_run = jnp.cumsum(log_keep, axis=1)
    log_last = log_run[:, -1]
    q_scaled = query_f * jnp.exp(log_run)
    k_scaled = key_f * jnp.exp(-log_run)
    k_carry = key_f * jnp.exp(log_last[:, None] - log_run)
    causal = jnp.tril(jnp.ones((BLOCK, BLOCK), bool))
    scores = jnp.einsum("nthk,nshk->nhts", q_scaled, k_scaled, precision=PRECISE)
    scores = jnp.where(causal, scores, 0.0)
    within = jnp.einsum("nhts,nshv->nthv", scores, value_f, precision=PRECISE)
    push_state = jnp.einsum("nshk,nshv->nhkv", k_carry, value_f, precision=PRECISE)
    keep_block = jnp.exp(log_last)
    keep_run, state_run = lax.associative_scan(link_states, (keep_block, push_state), axis=0)
    before = jnp.concatenate([jnp.zeros_like(state_run[:1]), state_run[:-1]], axis=0)
    keep_before = jnp.concatenate([jnp.ones_like(keep_run[:1]), keep_run[:-1]], axis=0)
    carried = jnp.einsum("nthk,nhkv->nthv", q_scaled, before, precision=PRECISE)
    return (within + carried, q_scaled * keep_before[:, None], keep_run[-1], state_run[-1])


def head_norm(mixer_out, head_gain):
    scale = lax.rsqrt(jnp.mean(mixer_out * mixer_out, axis=-1, keepdims=True) + NORM_EPS)
    return (mixer_out * scale * head_gain).astype(jnp.bfloat16)


def expert_mlp(slot_rows, w_gate, w_up, w_down):
    gate_part = jnp.einsum("serd,edf->serf", slot_rows, w_gate, preferred_element_type=jnp.float32)
    up_part = jnp.einsum("serd,edf->serf", slot_rows, w_up, preferred_element_type=jnp.float32)
    act = (jax.nn.silu(gate_part) * up_part).astype(jnp.bfloat16)
    return jnp.einsum("serf,efd->serd", act, w_down, preferred_element_type=jnp.float32).astype(
        jnp.bfloat16
    )


def local(
    queries,
    forget_pre,
    values,
    out_gate,
    lower_bound,
    head_gain,
    residual,
    out_weight,
    ffn_gain,
    routing,
    route_weight,
    expert_gate,
    expert_up,
    expert_down,
):
    tok_rows = queries.shape[1]
    head_size = head_gain.shape[0]
    model_width = residual.shape[2]
    arrived = side_by_side((queries, forget_pre, values), "sp", 2, 1, 0)
    seq_rows = arrived[0].shape[1]
    own_heads = arrived[0].shape[2] // head_size
    log_keep, leak_rate = forget_terms(arrived[1], lower_bound)
    layout = (seq_rows // BLOCK, BLOCK, own_heads, head_size)
    mixer_out, _, _, _ = recurrence(
        arrived[0].astype(jnp.float32).reshape(layout),
        log_keep.reshape(layout),
        leak_rate.reshape(layout),
        arrived[2].astype(jnp.float32).reshape(layout),
    )
    normed = head_norm(mixer_out, head_gain).reshape(1, seq_rows, own_heads * head_size)
    normed = lax.all_to_all(normed, "sp", split_axis=1, concat_axis=2, tiled=True)
    gated_out = (normed.astype(jnp.float32) * jax.nn.silu(out_gate.astype(jnp.float32))).astype(
        jnp.bfloat16
    )
    columns = jnp.einsum(
        "ntc,cd->ntd",
        lax.all_gather(gated_out, "dp", axis=0, tiled=True),
        out_weight,
        preferred_element_type=jnp.float32,
    ).astype(jnp.bfloat16)
    projected = lax.all_to_all(columns, "dp", split_axis=0, concat_axis=2, tiled=True)
    hidden = (residual.astype(jnp.float32) + projected.astype(jnp.float32)).astype(jnp.bfloat16)
    hidden_f = hidden.astype(jnp.float32).reshape(tok_rows, model_width)
    moe_in = (
        hidden_f
        * lax.rsqrt(jnp.mean(hidden_f * hidden_f, axis=-1, keepdims=True) + NORM_EPS)
        * ffn_gain
    ).astype(jnp.bfloat16)
    top_count = routing.shape[2]
    local_experts = expert_gate.shape[0]
    span_sp = lax.axis_size("sp")
    span_dp = lax.axis_size("dp")
    experts = local_experts * span_sp * span_dp
    capacity = max(2, 5 * tok_rows * top_count // (4 * experts))
    chosen = routing.reshape(tok_rows * top_count)
    matches = (chosen[:, None] == jnp.arange(experts, dtype=jnp.int32)[None, :]).astype(jnp.int32)
    rank_in = jnp.sum((jnp.cumsum(matches, axis=0) - 1) * matches, axis=1)
    target = chosen * capacity + rank_in
    owners = jnp.arange(tok_rows * top_count, dtype=jnp.int32) // top_count
    slot_owner = jnp.full((experts * capacity,), tok_rows, jnp.int32).at[target].set(owners)
    padded = jnp.concatenate([moe_in, jnp.zeros((1, model_width), jnp.bfloat16)], axis=0)
    outgoing = padded[slot_owner].reshape(span_sp * span_dp, local_experts, capacity, model_width)
    results = expert_mlp(
        lax.all_to_all(outgoing, ("sp", "dp"), split_axis=0, concat_axis=0, tiled=True),
        expert_gate,
        expert_up,
        expert_down,
    )
    returned = cut_exchange(results, ("sp", "dp"), 2, 0, 0)
    returned = returned.reshape(experts * capacity, model_width)
    picked = returned[target].reshape(tok_rows, top_count, model_width)
    weights = route_weight.reshape(tok_rows, top_count)
    weighted = jnp.einsum("tkd,tk->td", picked.astype(jnp.float32), weights, precision=PRECISE)
    return (hidden_f + weighted).astype(jnp.bfloat16).reshape(1, tok_rows, model_width)


def solution(mesh):
    in_specs = (
        P("dp", "sp", None),
        P("dp", "sp", None),
        P("dp", "sp", None),
        P("dp", "sp", None),
        P("sp"),
        P(),
        P("dp", "sp", None),
        P(None, "dp"),
        P(),
        P("dp", "sp", None),
        P("dp", "sp", None),
        P(("sp", "dp"), None, None),
        P(("sp", "dp"), None, None),
        P(("sp", "dp"), None, None),
    )
    out_specs = P("dp", "sp", None)
    return jax.shard_map(local, mesh=mesh, in_specs=in_specs, out_specs=out_specs, check_vma=False)
```

profile of v0, /device:TPU:1, one launch (start us, length us, event | category | flops | bytes accessed | tf_op | source)
XLA Modules:
  0.0 487.1 jit_solution(11175909272694930865)
XLA Ops:
  6.5 2.5 copy.36
  9.0 3.6 copy.37
  12.6 3.6 copy.38
  16.2 5.8 %pad_maximum_fusion.1 = bf16[3,128,2048]{1,0,2:T(4,128)(2,1)} fusion(bf16[1,128,2048]{1,0,2:T(2,128)(2,1)} %copy.38, bf16[1,128,2048]{1,0,2:T(2,128)(2,1)} %copy.37, bf16[1,128,2048]{1,0,2:T(2,128)(2,1)S(1)} %copy.36), kind=kLoop, calls=%fused_computation.22 | loop fusion | flops 4718592 | bytes 3145728 | tf_op jit(solution)/shard_map/concatenate | solution.py:18
  22.0 8.6 %all-to-all-start = ((bf16[3,128,2048]{1,0,2:T(4,128)(2,1)}), bf16[3,128,2048]{1,0,2:T(4,128)(2,1)}, u32[]{:S(2)}, u32[]{:S(2)}) async-start(bf16[3,128,2048]{1,0,2:T(4,128)(2,1)} %pad_maximum_fusion.1), calls=%async_computation | async-start | bytes 4194304 | tf_op jit(solution)/shard_map/all_to_all | solution.py:21
  31.5 30.2 %all-to-all-done = bf16[3,128,2048]{1,0,2:T(4,128)(2,1)} async-done(((bf16[3,128,2048]{1,0,2:T(4,128)(2,1)}), bf16[3,128,2048]{1,0,2:T(4,128)(2,1)}, u32[]{:S(2)}, u32[]{:S(2)}) %all-to-all-start) | async-done | bytes 1572896 | tf_op jit(solution)/shard_map/all_to_all | solution.py:21
  61.6 4.1 copy.40
  65.8 1.6 fusion.60
  68.2 2.7 fusion.57
  73.9 5.7 %pad.76 = f32[16,1,128,128]{3,2,0,1:T(8,128)} pad(f32[8,1,128,128]{3,2,0,1:T(8,128)} %add.157, f32[]{:T(128)} %constant.25.clone.1), padding=1_0_1x0_0_0x0_0_0x0_0_0 | pad | bytes 1572868
  79.6 1.2 fusion.71
  81.7 5.7 %pad.49 = f32[15,1,128,128]{3,2,0,1:T(8,128)} pad(f32[8,1,128,128]{3,2,0,1:T(8,128)} %pad_maximum_fusion.2, f32[]{:T(128)} %constant.25.clone.1), padding=0_0_1x0_0_0x0_0_0x0_0_0 | pad | bytes 1507332 | tf_op jit(solution)/shard_map/slice | solution.py:76
  87.4 4.3 convolution_select_fusion
  93.3 1.7 multiply_reduce_fusion
  95.4 8.3 %copy.103 = bf16[1,2048,128]{2,0,1:T(2,128)(2,1)S(1)} copy(bf16[1,2048,128]{2,1,0:T(8,128)(2,1)S(1)} %bitcast.205) | data formatting | bytes 1048576 | tf_op jit(solution)/shard_map/reshape | solution.py:126
  104.3 12.3 %reduce.2 = bf16[2048,128]{1,0:T(8,128)(2,1)} reduce(bf16[2048,1,128]{2,1,0:T(2,128)(2,1)S(1)} %bitcast.201, bf16[]{:T(256)} %broadcast.230), dimensions={1}, to_apply=%bitcast.193.reduce_sub_computation | reduce | bytes 1048578
  116.6 1.2 reshape.381
  117.8 14.4 %all_to_all.48 = bf16[16,2,8192]{2,1,0:T(2,128)(2,1)} all-to-all(bf16[16,2,8192]{2,1,0:T(2,128)(2,1)S(1)} %reshape.381), channel_id=1, replica_groups=mesh['sp'=16,'dp'=8] {'sp'}, dimensions={0} | all-to-all | bytes 1048576 | tf_op jit(solution)/shard_map/all_to_all | solution.py:127
  132.1 2.2 reshape.382
  134.4 1.1 bitcast_convert_fusion
  137.4 31.0 %all-gather.2.cloned.1.call-done = bf16[8,128,2048]{2,1,0:T(8,128)(2,1)} async-done(((bf16[1,128,2048]{2,1,0:T(8,128)(2,1)}), bf16[8,128,2048]{2,1,0:T(8,128)(2,1)}) %all-gather.2.cloned.1.call-update) | async-done | bytes 4194320 | tf_op jit(solution)/shard_map/all_gather | solution.py:133
  168.5 5.5 %fusion.16 = bf16[8,128,512]{2,1,0:T(8,128)(2,1)} fusion(bf16[8,128,2048]{2,1,0:T(8,128)(2,1)} %all-gather.2.cloned.1.call-done, bf16[2048,512]{1,0:T(8,128)(2,1)S(1)} %copy-done), kind=kOutput, calls=%fused_computation.27 | convolution fusion | flops 2148007936 | bytes 7340032 | tf_op jit(solution)/shard_map/ntc,cd->ntd/dot_general | solution.py:131
  174.0 3.7 all-to-all-start.2
  178.2 2.4 scatter_custom_fusion
  180.7 12.0 %all-to-all-done.2 = bf16[8,128,512]{2,1,0:T(8,128)(2,1)S(1)} async-done(((bf16[8,128,512]{2,1,0:T(8,128)(2,1)}), bf16[8,128,512]{2,1,0:T(8,128)(2,1)S(1)}, u32[]{:S(2)}, u32[]{:S(2)}) %all-to-all-start.2) | async-done | bytes 1048608 | tf_op jit(solution)/shard_map/all_to_all | solution.py:137
  193.0 1.8 copy.46
  194.8 1.9 copy.47
  196.8 1.6 fusion.10
  198.9 5.5 %gather_fusion = bf16[640,4096]{1,0:T(8,128)(2,1)} fusion(bf16[129,4096]{1,0:T(8,128)(2,1)S(1)} %concatenate.26, s32[1024]{0:T(1024)S(1)} %pad_clamp_fusion.1), kind=kCustom, calls=%fused_computation | custom fusion | bytes 10488320 | tf_op jit(solution)/shard_map/gather | solution.py:158
  204.3 8.4 %reshape.331 = bf16[128,1,5,4096]{3,2,0,1:T(8,128)(2,1)} reshape(bf16[640,4096]{1,0:T(8,128)(2,1)} %gather_fusion) | data formatting | bytes 10485760 | tf_op jit(solution)/shard_map/reshape | solution.py:158
  212.7 106.0 %all_to_all.49 = bf16[128,1,5,4096]{3,2,1,0:T(8,128)(2,1)S(1)} all-to-all(bf16[128,1,5,4096]{3,2,1,0:T(8,128)(2,1)} %bitcast.194), channel_id=1, replica_groups=mesh['sp'=16,'dp'=8] {'sp','dp'}, dimensions={0} | all-to-all | bytes 10485760 | tf_op jit(solution)/shard_map/all_to_all | solution.py:160
  318.8 5.8 %fusion.19 = f32[128,1,5,512]{3,0,2,1:T(8,128)S(1)} fusion(bf16[1,4096,512]{2,1,0:T(8,128)(2,1)S(1)} %copy-done.15, bf16[128,1,5,4096]{3,2,1,0:T(8,128)(2,1)S(1)} %all_to_all.49), kind=kOutput, calls=%fused_computation.28 | convolution fusion | flops 2684354560 | bytes 10747904 | tf_op jit(solution)/shard_map/serd,edf->serf/dot_general | solution.py:88
  324.6 6.2 %fusion.40 = bf16[128,5,512]{2,0,1:T(8,128)(2,1)S(1)} fusion(bf16[1,4096,512]{2,1,0:T(8,128)(2,1)S(1)} %copy-done.16, bf16[128,1,5,4096]{3,2,1,0:T(8,128)(2,1)S(1)} %all_to_all.49, f32[128,1,5,512]{3,0,2,1:T(8,128)S(1)} %fusion.19), kind=kOutput, calls=%fused_computation.37 | convolution fusion | flops 2686320640 | bytes 11403264 | tf_op jit(solution)/shard_map/serd,edf->serf/dot_general | solution.py:89
  330.8 3.2 fusion
  334.0 2.3 copy-done.2
  336.5 3.6 copy.55
  340.1 4.4 all-to-all-start.4
  344.5 1.9 slice-done
  346.4 4.7 copy.56
  351.0 23.7 %all-to-all-done.4 = bf16[128,1,1,2,4096]{4,3,2,1,0:T(2,128)(2,1)S(1)} async-done(((bf16[128,1,1,2,4096]{4,3,2,1,0:T(2,128)(2,1)}), bf16[128,1,1,2,4096]{4,3,2,1,0:T(2,128)(2,1)S(1)}, u32[]{:S(2)}, u32[]{:S(2)}) %all-to-all-start.4) | async-done | bytes 2097184 | tf_op jit(solution)/shard_map/all_to_all | solution.py:50
  374.7 6.3 %all-to-all-start.5 = ((bf16[128,1,1,3,4096]{4,3,2,1,0:T(4,128)(2,1)}), bf16[128,1,1,3,4096]{4,3,2,1,0:T(4,128)(2,1)}, u32[]{:S(2)}, u32[]{:S(2)}) async-start(bf16[128,1,1,3,4096]{4,3,2,1,0:T(4,128)(2,1)} %copy.56), calls=%async_computation.5 | async-start | bytes 8388608 | tf_op jit(solution)/shard_map/all_to_all | solution.py:50
  381.2 52.6 %all-to-all-done.5 = bf16[128,1,1,3,4096]{4,3,2,1,0:T(4,128)(2,1)} async-done(((bf16[128,1,1,3,4096]{4,3,2,1,0:T(4,128)(2,1)}), bf16[128,1,1,3,4096]{4,3,2,1,0:T(4,128)(2,1)}, u32[]{:S(2)}, u32[]{:S(2)}) %all-to-all-start.5) | async-done | bytes 3145760 | tf_op jit(solution)/shard_map/all_to_all | solution.py:50
  433.7 7.7 %pad_maximum_fusion = bf16[128,1,1,5,4096]{4,3,2,1,0:T(8,128)(2,1)} fusion(bf16[128,1,1,3,4096]{4,3,2,1,0:T(4,128)(2,1)} %all-to-all-done.5, bf16[128,1,1,2,4096]{4,3,2,1,0:T(2,128)(2,1)S(1)} %all-to-all-done.4), kind=kLoop, calls=%fused_computation.3 | loop fusion | flops 10485760 | bytes 10485760 | tf_op jit(solution)/shard_map/concatenate | solution.py:51
  441.5 8.7 %reshape_reshape.3 = bf16[640,4096]{1,0:T(8,128)(2,1)} reshape(bf16[128,1,1,5,4096]{4,3,2,1,0:T(8,128)(2,1)} %pad_maximum_fusion) | data formatting | bytes 10485760 | tf_op jit(solution)/shard_map/reshape;reshape | solution.py:166
  450.1 11.7 %gather_fusion.1 = bf16[512,4096]{1,0:T(8,128)(2,1)} fusion(bf16[640,4096]{1,0:T(8,128)(2,1)} %reshape_reshape.3, s32[1024]{0:T(1024)S(1)} %pad_clamp_fusion), kind=kCustom, calls=%fused_computation.1 | custom fusion | bytes 8390656 | tf_op jit(solution)/shard_map/gather | solution.py:167
  461.9 7.2 %reshape.338 = bf16[128,4,4096]{2,1,0:T(4,128)(2,1)} reshape(bf16[512,4096]{1,0:T(8,128)(2,1)} %gather_fusion.1) | data formatting | bytes 8388608 | tf_op jit(solution)/shard_map/reshape | solution.py:167
  469.1 8.6 %fusion.89 = f32[128,1,4096]{2,1,0:T(1,128)S(1)} fusion(bf16[128,4,4096]{2,1,0:T(4,128)(2,1)} %reshape.338, f32[128,4,1]{1,2,0:T(1,128)S(1)} %copy.58), kind=kOutput, calls=%fused_computation.128 | convolution fusion | flops 25165824 | bytes 6293504 | tf_op jit(solution)/shard_map/tkd,tk->td/dot_general | solution.py:169
  477.8 2.2 fusion.50
  (106 shorter events, 11.2 us)
Async XLA Ops:
  6.5 162.0 %copy-start = (bf16[2048,512]{1,0:T(8,128)(2,1)S(1)}, bf16[2048,512]{1,0:T(8,128)(2,1)}, u32[]{:S(2)}) copy-start(bf16[2048,512]{1,0:T(8,128)(2,1)} %param.21) | copy-start | bytes 6291460
  22.0 9.4 %copy-start.18 = (f32[128]{0:T(128)S(1)}, f32[128]{0:T(128)}, u32[]{:S(2)}) copy-start(f32[128]{0:T(128)} %param.18) | copy-start | bytes 1540
  22.0 39.6 %all-to-all-start = ((bf16[3,128,2048]{1,0,2:T(4,128)(2,1)}), bf16[3,128,2048]{1,0,2:T(4,128)(2,1)}, u32[]{:S(2)}, u32[]{:S(2)}) async-start(bf16[3,128,2048]{1,0,2:T(4,128)(2,1)} %pad_maximum_fusion.1), calls=%async_computation | async-start | bytes 4194304 | tf_op jit(solution)/shard_map/all_to_all | solution.py:21
  30.6 137.9 %all-gather.2.cloned.1.call-start = ((), (), s32[]{:S(2)}) async-start(), calls=%async_computation.6 | async-start | bytes 4718592 | tf_op jit(solution)/shard_map/all_gather | solution.py:133
  68.0 2.9 copy-start.4
  70.9 1.0 copy-start.8
  79.6 7.8 %copy-start.11 = (pred[128,128]{1,0:T(8,128)(4,1)S(1)}, pred[128,128]{1,0:T(8,128)(4,1)}, u32[]{:S(2)}) copy-start(pred[128,128]{1,0:T(8,128)(4,1)} %iota_compare_fusion.3) | copy-start | bytes 49156
  80.9 6.6 %copy-start.5 = (f32[16,128,1,128]{3,0,1,2:T(8,128)S(1)}, f32[16,128,1,128]{3,0,1,2:T(8,128)}, u32[]{:S(2)}) copy-start(f32[16,128,1,128]{3,0,1,2:T(8,128)} %copy-done.4) | copy-start | bytes 3145732
  87.4 4.3 copy-start.3
  91.7 1.2 copy-start.6
  91.7 1.5 copy-start.7
  93.3 1.7 copy-start.14
  134.4 1.2 copy-start.9
  134.4 2.3 copy-start.12
  174.0 18.7 %all-to-all-start.2 = ((bf16[8,128,512]{2,1,0:T(8,128)(2,1)}), bf16[8,128,512]{2,1,0:T(8,128)(2,1)S(1)}, u32[]{:S(2)}, u32[]{:S(2)}) async-start(bf16[8,128,512]{2,1,0:T(8,128)(2,1)} %fusion.16), calls=%async_computation.2 | async-start | bytes 2097152 | tf_op jit(solution)/shard_map/all_to_all | solution.py:137
  196.7 1.7 copy-start.10
  212.7 106.0 %copy-start.15 = (bf16[1,4096,512]{2,1,0:T(8,128)(2,1)S(1)}, bf16[1,4096,512]{2,1,0:T(8,128)(2,1)}, u32[]{:S(2)}) copy-start(bf16[1,4096,512]{2,1,0:T(8,128)(2,1)} %param.25) | copy-start | bytes 12582916
  318.8 5.8 %copy-start.16 = (bf16[1,4096,512]{2,1,0:T(8,128)(2,1)S(1)}, bf16[1,4096,512]{2,1,0:T(8,128)(2,1)}, u32[]{:S(2)}) copy-start(bf16[1,4096,512]{2,1,0:T(8,128)(2,1)} %param.26) | copy-start | bytes 12582916
  324.6 6.2 %copy-start.17 = (bf16[1,512,4096]{2,1,0:T(8,128)(2,1)S(1)}, bf16[1,512,4096]{2,1,0:T(8,128)(2,1)}, u32[]{:S(2)}) copy-start(bf16[1,512,4096]{2,1,0:T(8,128)(2,1)} %param.27) | copy-start | bytes 12582916
  334.0 2.3 copy-start.2
  340.1 34.6 %all-to-all-start.4 = ((bf16[128,1,1,2,4096]{4,3,2,1,0:T(2,128)(2,1)}), bf16[128,1,1,2,4096]{4,3,2,1,0:T(2,128)(2,1)S(1)}, u32[]{:S(2)}, u32[]{:S(2)}) async-start(bf16[128,1,1,2,4096]{4,3,2,1,0:T(2,128)(2,1)} %copy.55), calls=%async_computation.4 | async-start | bytes 4194304 | tf_op jit(solution)/shard_map/all_to_all | solution.py:50
  344.5 1.9 slice-start
  351.0 30.0 %copy-start.13 = (f32[1,128,4]{1,2,0:T(4,128)S(1)}, f32[1,128,4]{1,2,0:T(4,128)}, u32[]{:S(2)}) copy-start(f32[1,128,4]{1,2,0:T(4,128)} %param.24) | copy-start | bytes 6148
  374.7 59.0 %all-to-all-start.5 = ((bf16[128,1,1,3,4096]{4,3,2,1,0:T(4,128)(2,1)}), bf16[128,1,1,3,4096]{4,3,2,1,0:T(4,128)(2,1)}, u32[]{:S(2)}, u32[]{:S(2)}) async-start(bf16[128,1,1,3,4096]{4,3,2,1,0:T(4,128)(2,1)} %copy.56), calls=%async_computation.5 | async-start | bytes 8388608 | tf_op jit(solution)/shard_map/all_to_all | solution.py:50
  469.1 10.9 %copy-start.1 = (bf16[2048,512]{1,0:T(8,128)(2,1)S(1)}, bf16[2048,512]{1,0:T(8,128)(2,1)}, u32[]{:S(2)}) copy-start(bf16[2048,512]{1,0:T(8,128)(2,1)} %param.21) | copy-start | bytes 6291460
Sparse Core Ops, SparseCore 0:
  136.8 31.6 all-gather.1
where the time goes:
time: 492 us; the launch traced here: 487 us
  waiting for transfers between devices  150 us (30%)
  blocking collectives  120 us (24%)
  local copies, waits for them, and re-layouts  101 us (21%)
  other arithmetic  40.1 us (8%)
  matrix products  38.7 us (8%)
  starting transfers between devices  23.2 us (5%)
  between operations  14.2 us (3%)
    all_to_all x1, blocking collectives, local(): lax.all_to_all(outgoing, ('sp', 'dp'), split_axis=0, concat_axis=0, tiled...  106 us
    all_to_all x2, waiting for transfers between devices, cut_exchange(): lax.all_to_all(piece, axis, split_axis=0, concat_axis=0, tiled=True)  76.3 us
    all_gather x1, waiting for transfers between devices, local(): lax.all_gather(gated_out, 'dp', axis=0, tiled=True)  31 us
    all_to_all x1, waiting for transfers between devices, side_by_side(): lax.all_to_all(both, axis, split_axis=split_dim, concat_axis=concat_dim,...  30.2 us
    unnamed x46, local copies, waits for them, and re-layouts  23.6 us
    all_to_all x1, blocking collectives, local(): lax.all_to_all(normed, 'sp', split_axis=1, concat_axis=2, tiled=True)  14.4 us
    unnamed x1, other arithmetic  12.3 us
    all_to_all x1, waiting for transfers between devices, local(): lax.all_to_all(columns, 'dp', split_axis=0, concat_axis=2, tiled=True)  12 us
  transfers between devices with their start and end apart: 5, of which 5 were waited for; matrix products, arithmetic and copies ran while one was open for 2% of the time, Pallas kernels for 0%

commit v1 on v0

v1 whole, which is shorter than its diff:
```python
import functools

import jax
import jax.numpy as jnp
from jax import lax
from jax.experimental import pallas as pl
from jax.experimental.pallas import tpu as pltpu
from jax.sharding import PartitionSpec as P

NORM_EPS = 1e-06
LANES = 128
CAPACITY = 5
BF16 = jnp.bfloat16
F32 = jnp.float32
MSG_PAD = 16


def dot(a, b, dims=((1,), (0,)), precision=None):
    return lax.dot_general(
        a, b, (dims, ((), ())), preferred_element_type=F32, precision=precision
    )


def gate_terms(forget_ref, bound_ref):
    leak = (1.0 - bound_ref[...]) * jax.nn.sigmoid(-forget_ref[...].astype(F32))
    log_keep = jnp.log1p(-leak)
    rows = log_keep.shape[0]
    at = lax.broadcasted_iota(jnp.int32, (rows, rows), 0)
    of = lax.broadcasted_iota(jnp.int32, (rows, rows), 1)
    causal = of <= at
    log_run = dot(jnp.where(causal, 1.0, 0.0), log_keep, precision=lax.Precision.HIGHEST)
    return leak, log_run, causal


def push_kernel(forget_ref, value_ref, bound_ref, message_ref):
    leak, log_run, _ = gate_terms(forget_ref, bound_ref)
    rows, size = leak.shape
    log_last = log_run[rows - 1 : rows, :]
    carry = leak * jnp.exp(log_last - log_run)
    push = dot(value_ref[...], carry.astype(BF16), ((0,), (0,)))
    message_ref[0, 0:size, :] = push.astype(BF16)
    keep = jnp.exp(log_last)
    high = keep.astype(BF16)
    low = (keep - high.astype(F32)).astype(BF16)
    row = lax.broadcasted_iota(jnp.int32, (MSG_PAD, size), 0)
    tail = jnp.where(row == 0, high.astype(F32), jnp.where(row == 1, low.astype(F32), 0.0))
    message_ref[0, size : size + MSG_PAD, :] = tail.astype(BF16)


def scan_kernel(message_ref, before_ref):
    blocks, _, size = message_ref.shape
    state = jnp.zeros((size, size), F32)
    for n in range(blocks):
        before_ref[n] = state.astype(BF16)
        tail = message_ref[n, size : size + MSG_PAD, :].astype(F32)
        keep = tail[0:1, :] + tail[1:2, :]
        state = keep * state + message_ref[n, 0:size, :].astype(F32)


def mix_kernel(
    query_ref, forget_ref, value_ref, gate_ref, bound_ref, before_ref, gain_ref, out_ref
):
    leak, log_run, causal = gate_terms(forget_ref, bound_ref)
    q_scaled = (query_ref[...].astype(F32) * jnp.exp(log_run)).astype(BF16)
    k_scaled = (leak * jnp.exp(-log_run)).astype(BF16)
    scores = jnp.where(causal, dot(q_scaled, k_scaled, ((1,), (1,))), 0.0)
    mix = dot(scores.astype(BF16), value_ref[...])
    mix = mix + dot(q_scaled, before_ref[0], ((1,), (1,)))
    scale = lax.rsqrt(jnp.mean(mix * mix, axis=-1, keepdims=True) + NORM_EPS)
    normed = (mix * scale * gain_ref[...]).astype(BF16)
    u = gate_ref[...].astype(F32)
    out_ref[...] = (normed.astype(F32) * (u / (1.0 + jnp.exp(-u)))).astype(BF16)


def project_kernel(
    slot_ref,
    gated_ref,
    weight_ref,
    residual_ref,
    gain_ref,
    outgoing_ref,
    hidden_ref,
    wide_ref,
    square_ref,
    moe_ref,
    keep_ref,
):
    step = pl.program_id(0)
    tokens, columns = residual_ref.shape
    width = wide_ref.shape[1]
    pieces = width // LANES
    projected = dot(gated_ref[...], weight_ref[0]).astype(BF16)
    hidden = (residual_ref[...].astype(F32) + projected.astype(F32)).astype(BF16).astype(F32)
    at = pl.multiple_of(step * columns, columns)
    wide_ref[:, pl.ds(at, columns)] = hidden
    squares = jnp.sum(hidden * hidden, axis=-1, keepdims=True)

    @pl.when(step == 0)
    def _():
        square_ref[...] = jnp.zeros_like(square_ref)

    square_ref[...] += jnp.broadcast_to(squares, square_ref.shape)

    @pl.when(step == pl.num_programs(0) - 1)
    def _():
        scale = lax.rsqrt(square_ref[...] / width + NORM_EPS)
        for c in range(pieces):
            part = wide_ref[:, c * LANES : (c + 1) * LANES]
            keep_ref[pl.ds(c, tokens, stride=pieces), :] = part
            gain = gain_ref[:, c * LANES : (c + 1) * LANES]
            moe_ref[pl.ds(c, tokens, stride=pieces), :] = part * scale * gain

        def keep_row(t, _):
            row = pl.multiple_of(t * pieces, pieces)
            hidden_ref[t] = keep_ref[pl.ds(row, pieces), :].astype(BF16)
            return 0

        lax.fori_loop(0, tokens, keep_row, 0, unroll=4)

        def fill_slot(s, _):
            row = pl.multiple_of(slot_ref[s] * pieces, pieces)
            outgoing_ref[s] = moe_ref[pl.ds(row, pieces), :].astype(BF16)
            return 0

        lax.fori_loop(0, outgoing_ref.shape[0], fill_slot, 0, unroll=8)


def expert_kernel(rows_ref, gate_ref, up_ref, down_ref, out_ref, wide_ref, x_ref):
    rows, pieces, _ = rows_ref.shape
    wide_ref[...] = rows_ref[...].astype(F32).reshape(rows * pieces, LANES)
    for c in range(pieces):
        x_ref[:, c * LANES : (c + 1) * LANES] = wide_ref[
            pl.ds(c, rows, stride=pieces), :
        ].astype(BF16)
    x = x_ref[...]
    gate = dot(x, gate_ref[0])
    up = dot(x, up_ref[0])
    act = (gate / (1.0 + jnp.exp(-gate)) * up).astype(BF16)
    for c in range(pieces):
        part = dot(act, down_ref[0, :, c * LANES : (c + 1) * LANES])
        wide_ref[pl.ds(c, rows, stride=pieces), :] = part
    out_ref[...] = wide_ref[...].reshape(rows, pieces, LANES).astype(BF16)


def combine_kernel(target_ref, weight_ref, back_ref, hidden_ref, out_ref, wide_ref):
    tokens, pieces, _ = hidden_ref.shape
    top = target_ref.shape[0] // tokens

    def one(t, _):
        total = jnp.zeros((pieces, LANES), F32)
        for j in range(top):
            i = t * top + j
            total = total + weight_ref[i] * back_ref[target_ref[i]].astype(F32)
        row = pl.multiple_of(t * pieces, pieces)
        wide_ref[pl.ds(row, pieces), :] = hidden_ref[t].astype(F32) + total
        return 0

    lax.fori_loop(0, tokens, one, 0, unroll=4)
    for c in range(pieces):
        out_ref[:, c * LANES : (c + 1) * LANES] = wide_ref[
            pl.ds(c, tokens, stride=pieces), :
        ].astype(BF16)


def whole(shape, space=None):
    if space is None:
        return pl.BlockSpec(shape, lambda *_: (0,) * len(shape))
    return pl.BlockSpec(memory_space=space)


def cost(flops, moved):
    return pl.CostEstimate(flops=int(flops), bytes_accessed=int(moved), transcendentals=0)


def slots_of(chosen, experts, capacity, tokens, top_count):
    matches = (chosen[:, None] == jnp.arange(experts, dtype=jnp.int32)[None, :]).astype(jnp.int32)
    rank_in = jnp.sum((jnp.cumsum(matches, axis=0) - 1) * matches, axis=1)
    target = chosen * capacity + rank_in
    owners = jnp.arange(tokens * top_count, dtype=jnp.int32) // top_count
    slot_owner = jnp.zeros((experts * capacity,), jnp.int32).at[target].set(owners)
    return target, slot_owner


def local(
    queries,
    forget_pre,
    values,
    out_gate,
    lower_bound,
    head_gain,
    residual,
    out_weight,
    ffn_gain,
    routing,
    route_weight,
    expert_gate,
    expert_up,
    expert_down,
):
    tokens = queries.shape[1]
    channels = queries.shape[2]
    size = head_gain.shape[0]
    heads = channels // size
    width = residual.shape[2]
    pieces = width // LANES
    top_count = routing.shape[2]
    span = lax.axis_size("sp") * lax.axis_size("dp")
    experts = expert_gate.shape[0] * span
    slots = experts * CAPACITY

    weights_all = lax.all_gather(out_weight, "dp")
    bound = lax.all_gather(lower_bound, "sp", tiled=True).reshape(1, channels)
    target, slot_owner = slots_of(
        routing.reshape(tokens * top_count), experts, CAPACITY, tokens, top_count
    )

    head_block = pl.BlockSpec((tokens, size), lambda h: (0, h))
    bound_block = pl.BlockSpec((1, size), lambda h: (0, h))
    q = queries.reshape(tokens, channels)
    f = forget_pre.reshape(tokens, channels)
    v = values.reshape(tokens, channels)
    g = out_gate.reshape(tokens, channels)
    message = pl.pallas_call(
        push_kernel,
        grid=(heads,),
        in_specs=[head_block, head_block, bound_block],
        out_specs=pl.BlockSpec((1, size + MSG_PAD, size), lambda h: (h, 0, 0)),
        out_shape=jax.ShapeDtypeStruct((heads, size + MSG_PAD, size), BF16),
        cost_estimate=cost(8e8, 2e6),
        name="push",
    )(f, v, bound)
    arrived = lax.all_to_all(message, "sp", split_axis=0, concat_axis=0, tiled=True)
    before = pl.pallas_call(
        scan_kernel,
        out_shape=jax.ShapeDtypeStruct((arrived.shape[0], size, size), BF16),
        cost_estimate=cost(1e8, 1e6),
        name="scan",
    )(arrived)
    before = lax.all_to_all(before, "sp", split_axis=0, concat_axis=0, tiled=True)
    gated = pl.pallas_call(
        mix_kernel,
        grid=(heads,),
        in_specs=[head_block] * 4
        + [
            bound_block,
            pl.BlockSpec((1, size, size), lambda h: (h, 0, 0)),
            pl.BlockSpec((1, size), lambda h: (0, 0)),
        ],
        out_specs=head_block,
        out_shape=jax.ShapeDtypeStruct((tokens, channels), BF16),
        cost_estimate=cost(1.2e9, 3e6),
        name="mix",
    )(q, f, v, g, bound, before, head_gain.reshape(1, size))

    columns = out_weight.shape[1]
    outgoing, hidden = pl.pallas_call(
        project_kernel,
        grid=(width // columns,),
        in_specs=[
            whole(None, pltpu.SMEM),
            pl.BlockSpec((tokens, channels), lambda i: (0, 0)),
            pl.BlockSpec((1, channels, columns), lambda i: (i, 0, 0)),
            pl.BlockSpec((tokens, columns), lambda i: (0, i)),
            pl.BlockSpec((1, width), lambda i: (0, 0)),
        ],
        out_specs=[
            pl.BlockSpec((slots, pieces, LANES), lambda i: (0, 0, 0)),
            pl.BlockSpec((tokens, pieces, LANES), lambda i: (0, 0, 0)),
        ],
        out_shape=[
            jax.ShapeDtypeStruct((slots, pieces, LANES), BF16),
            jax.ShapeDtypeStruct((tokens, pieces, LANES), BF16),
        ],
        scratch_shapes=[
            pltpu.VMEM((tokens, width), F32),
            pltpu.VMEM((tokens, LANES), F32),
            pltpu.VMEM((tokens * pieces, LANES), F32),
            pltpu.VMEM((tokens * pieces, LANES), F32),
        ],
        cost_estimate=cost(2.2e9, 24e6),
        compiler_params=pltpu.CompilerParams(vmem_limit_bytes=40 * 2**20),
        name="project",
    )(
        slot_owner,
        gated,
        weights_all,
        residual.reshape(tokens, width),
        ffn_gain.reshape(1, width),
    )

    exchange = functools.partial(
        lax.all_to_all, axis_name=("sp", "dp"), split_axis=0, concat_axis=0, tiled=True
    )
    chunk = (span, CAPACITY * pieces, LANES)
    rows_in = exchange(outgoing.reshape(chunk)).reshape(slots, pieces, LANES)
    hidden_units = expert_gate.shape[2]
    rows = tokens
    row_block = pl.BlockSpec((rows, pieces, LANES), lambda i: (i, 0, 0))
    results = pl.pallas_call(
        expert_kernel,
        grid=(slots // rows,),
        in_specs=[
            row_block,
            pl.BlockSpec((1, width, hidden_units), lambda i: (0, 0, 0)),
            pl.BlockSpec((1, width, hidden_units), lambda i: (0, 0, 0)),
            pl.BlockSpec((1, hidden_units, width), lambda i: (0, 0, 0)),
        ],
        out_specs=row_block,
        out_shape=jax.ShapeDtypeStruct((slots, pieces, LANES), BF16),
        scratch_shapes=[
            pltpu.VMEM((rows * pieces, LANES), F32),
            pltpu.VMEM((rows, width), BF16),
        ],
        cost_estimate=cost(8e9, 24e6),
        compiler_params=pltpu.CompilerParams(vmem_limit_bytes=48 * 2**20),
        name="expert",
    )(rows_in, expert_gate, expert_up, expert_down)
    back = exchange(results.reshape(chunk)).reshape(slots, pieces, LANES)
    out = pl.pallas_call(
        combine_kernel,
        in_specs=[
            whole(None, pltpu.SMEM),
            whole(None, pltpu.SMEM),
            whole(None, pltpu.VMEM),
            whole(None, pltpu.VMEM),
        ],
        out_specs=whole(None, pltpu.VMEM),
        out_shape=jax.ShapeDtypeStruct((tokens, width), BF16),
        scratch_shapes=[pltpu.VMEM((tokens * pieces, LANES), F32)],
        cost_estimate=cost(4e8, 8e6),
        compiler_params=pltpu.CompilerParams(vmem_limit_bytes=32 * 2**20),
        name="combine",
    )(target, route_weight.reshape(tokens * top_count), back, hidden)
    return out.reshape(1, tokens, width)


def solution(mesh):
    in_specs = (
        P("dp", "sp", None),
        P("dp", "sp", None),
        P("dp", "sp", None),
        P("dp", "sp", None),
        P("sp"),
        P(),
        P("dp", "sp", None),
        P(None, "dp"),
        P(),
        P("dp", "sp", None),
        P("dp", "sp", None),
        P(("sp", "dp"), None, None),
        P(("sp", "dp"), None, None),
        P(("sp", "dp"), None, None),
    )
    out_specs = P("dp", "sp", None)
    return jax.shard_map(local, mesh=mesh, in_specs=in_specs, out_specs=out_specs, check_vma=False)
```

time: 492 us -> 304 us (0.62)
  local copies, waits for them, and re-layouts: 101 us -> 6.02 us
  Pallas kernels: 0 us -> 78.9 us
  waiting for transfers between devices: 150 us -> 94.8 us
  other arithmetic: 40.1 us -> 0.56 us
  matrix products: 38.7 us -> 0 us
  blocking collectives: 120 us -> 92.6 us
  starting transfers between devices: 23.2 us -> 14 us
    pallas_call x0 -> x6, Pallas kernels: none -> 78.9 us  [the longest x1 31.4 us: local(): pl.pallas_call(expert_kernel, grid=(slots // rows,), in_specs=[row_block,...]
    all_to_all x2 -> x1, blocking collectives: 120 us -> 72.1 us  [local(): rows_in = exchange(outgoing.reshape(chunk)).reshape(slots, pieces, LANES)]
    all_to_all x4 -> x3, waiting for transfers between devices: 118 us -> 78.5 us  [the longest x1 63.9 us: local(): back = exchange(results.reshape(chunk)).reshape(slots, pieces, LANES)]
    dot_general x9 -> x0, matrix products: 38.7 us -> none  [the longest x1 8.65 us: local(): jnp.einsum('tkd,tk->td', picked.astype(jnp.float32), weights, precision=P...]
    reshape x4 -> x2, local copies, waits for them, and re-layouts: 24.1 us -> 0.21 us  [the longest x1 0.11 us: local(): route_weight.reshape(tokens * top_count)]
    unnamed x46 -> x18, local copies, waits for them, and re-layouts: 23.6 us -> 2.9 us
    all_gather x0 -> x1, blocking collectives: none -> 20.6 us  [local(): bound = lax.all_gather(lower_bound, 'sp', tiled=True).reshape(1, channels)]
    gather x2 -> x0, local copies, waits for them, and re-layouts: 17.2 us -> none  [the longest x1 11.7 us: local(): picked = returned[target].reshape(tok_rows, top_count, model_width)]
  transfers between devices with their start and end apart: 5 -> 4, of which waited for: 5 -> 4; matrix products, arithmetic and copies ran while one was open for 2% -> 1% of each run, Pallas kernels for 0% -> 9%
where the time goes in v1:
time: 304 us; the launch traced here: 300 us
  waiting for transfers between devices  94.8 us (31%)
  blocking collectives  92.6 us (30%)
  Pallas kernels  78.9 us (26%)
  starting transfers between devices  14 us (5%)
  between operations  13.5 us (4%)
  local copies, waits for them, and re-layouts  6.02 us (2%)
    all_to_all x1, blocking collectives, local(): rows_in = exchange(outgoing.reshape(chunk)).reshape(slots, pieces, LANES)  72.1 us
    all_to_all x1, waiting for transfers between devices, local(): back = exchange(results.reshape(chunk)).reshape(slots, pieces, LANES)  63.9 us
    pallas_call x1, Pallas kernels, local(): pl.pallas_call(expert_kernel, grid=(slots // rows,), in_specs=[row_block,...  31.4 us
    all_gather x1, blocking collectives, local(): bound = lax.all_gather(lower_bound, 'sp', tiled=True).reshape(1, channels)  20.6 us
    all_gather x1, waiting for transfers between devices, local(): weights_all = lax.all_gather(out_weight, 'dp')  15.6 us
    pallas_call x1, Pallas kernels, local(): pl.pallas_call(project_kernel, grid=(width // columns,), in_specs=[whole(...  14.9 us
    pallas_call x1, Pallas kernels, local(): pl.pallas_call(mix_kernel, grid=(heads,), in_specs=[head_block] * 4 + [bo...  13.3 us
    pallas_call x1, Pallas kernels, local(): pl.pallas_call(push_kernel, grid=(heads,), in_specs=[head_block, head_blo...  10.9 us
  transfers between devices with their start and end apart: 4, of which 4 were waited for; matrix products, arithmetic and copies ran while one was open for 1% of the time, Pallas kernels for 9%

profile of v1, /device:TPU:1, one launch (start us, length us, event | category | flops | bytes accessed | tf_op | source)
XLA Modules:
  0.0 300.5 jit_solution(5281686672770915327)
XLA Ops:
  6.5 0.0 copy-start.6
  6.5 0.0 all-gather.4.cloned.1.call-start
  6.5 0.7 all-gather.4.cloned.1.call-update
  7.3 20.6 %all-gather.1 = f32[16,1,128]{2,1,0:T(1,128)} all-gather(f32[1,1,128]{2,1,0:T(1,128)} %bitcast.36), channel_id=1, replica_groups=mesh['sp'=16,'dp'=8] {'sp'}, dimensions={0}, use_global_device_ids=true | all-gather | bytes 8704 | tf_op jit(solution)/shard_map/all_gather | solution.py:212
  27.8 10.9 %push.1 = bf16[16,144,128]{2,1,0:T(8,128)(2,1)} custom-call(bf16[128,2048]{1,0:T(8,128)(2,1)} %bitcast.38, bf16[128,2048]{1,0:T(8,128)(2,1)} %bitcast.40, f32[1,2048]{1,0:T(1,128)} %bitcast.33), custom_call_target="tpu_custom_call" | custom-call | flops 800000000 | bytes 2000000 | tf_op jit(solution)/shard_map/push/pallas_call | solution.py:223
  38.7 0.0 copy-start
  38.7 0.0 copy-start.2
  38.7 4.5 %all-to-all-start = ((bf16[16,144,128]{2,1,0:T(8,128)(2,1)}), bf16[16,144,128]{2,1,0:T(8,128)(2,1)S(1)}, u32[]{:S(2)}, u32[]{:S(2)}) async-start(bf16[16,144,128]{2,1,0:T(8,128)(2,1)} %push.1), calls=%async_computation | async-start | bytes 1179648 | tf_op jit(solution)/shard_map/all_to_all | solution.py:232
  43.2 0.0 copy-done.6
  43.2 0.1 copy.21
  43.3 0.1 eq.26
  43.5 0.1 copy.23
  43.6 0.2 fusion.1
  43.8 0.1 add_add_fusion
  43.9 8.7 %all-to-all-done.message_ref = bf16[16,144,128]{2,1,0:T(8,128)(2,1)S(1)} async-done(((bf16[16,144,128]{2,1,0:T(8,128)(2,1)}), bf16[16,144,128]{2,1,0:T(8,128)(2,1)S(1)}, u32[]{:S(2)}, u32[]{:S(2)}) %all-to-all-start) | async-done | bytes 589856 | tf_op jit(solution)/shard_map/all_to_all | solution.py:232
  52.6 0.0 copy-start.4
  52.6 0.8 copy-done.4
  53.4 2.0 scan.1
  55.4 3.6 %all-to-all-start.1 = ((bf16[16,128,128]{2,1,0:T(8,128)(2,1)}), bf16[16,128,128]{2,1,0:T(8,128)(2,1)S(1)}, u32[]{:S(2)}, u32[]{:S(2)}) async-start(bf16[16,128,128]{2,1,0:T(8,128)(2,1)} %scan.1), calls=%async_computation.1 | async-start | bytes 1048576 | tf_op jit(solution)/shard_map/all_to_all | solution.py:239
  59.0 0.1 reshape.92
  59.1 0.1 copy.26
  59.2 0.1 mul.28
  59.3 0.2 fusion
  59.6 2.4 scatter_custom_fusion.slot_ref
  62.0 5.9 %all-to-all-done.1.before_ref = bf16[16,128,128]{2,1,0:T(8,128)(2,1)S(1)} async-done(((bf16[16,128,128]{2,1,0:T(8,128)(2,1)}), bf16[16,128,128]{2,1,0:T(8,128)(2,1)S(1)}, u32[]{:S(2)}, u32[]{:S(2)}) %all-to-all-start.1) | async-done | bytes 524320 | tf_op jit(solution)/shard_map/all_to_all | solution.py:239
  67.9 0.0 copy-start.5
  67.9 0.8 copy-done.5
  68.7 13.3 %mix.1.gated_ref = bf16[128,2048]{1,0:T(8,128)(2,1)} custom-call(bf16[128,2048]{1,0:T(8,128)(2,1)} %bitcast.37, bf16[128,2048]{1,0:T(8,128)(2,1)} %bitcast.39, bf16[128,2048]{1,0:T(8,128)(2,1)} %bitcast.41, bf16[128,2048]{1,0:T(8,128)(2,1)} %bitcast.42, f32[1,2048]{1,0:T(1,128)} %bitcast.34, bf16[16,128,128]{2,1,0:T(8,128)(2,1)} %copy-done.5, f32[1,128]{1,0:T(1,128)} %bitcast.43), custom_call_target="tpu_custom_call" | custom-call | flops 1200000000 | bytes 3000000 | tf_op jit(solution)/shard_map/mix/pallas_call | solution.py:240
  82.0 15.6 %all-gather.4.cloned.1.call-done = bf16[16384,512]{1,0:T(8,128)(2,1)} async-done(((bf16[2048,512]{1,0:T(8,128)(2,1)}), bf16[16384,512]{1,0:T(8,128)(2,1)}) %all-gather.4.cloned.1.call-update) | async-done | bytes 16777232 | tf_op jit(solution)/shard_map/all_gather | solution.py:211
  97.6 0.0 copy-done
  97.6 0.0 copy-done.2
  97.6 0.0 copy-start.1
  97.6 1.0 copy-done.1
  98.7 14.9 %project.1 = (bf16[640,32,128]{2,1,0:T(8,128)(2,1)S(1)}, bf16[128,32,128]{2,1,0:T(8,128)(2,1)S(1)}) custom-call(s32[640]{0:T(1024)S(1)} %scatter_custom_fusion.slot_ref, bf16[128,2048]{1,0:T(8,128)(2,1)S(1)} %copy-done.1, bf16[8,2048,512]{2,1,0:T(8,128)(2,1)} %bitcast.29, bf16[128,4096]{1,0:T(8,128)(2,1)S(1)} %bitcast.27, f32[1,4096]{1,0:T(1,128)S(1)} %bitcast.28), custom_call_target="tpu_custom_call" | custom-call | flops 2200000000 | bytes 24000000 | tf_op jit(solution)/shard_map/project/pallas_call | solution.py:256
  113.6 0.0 copy-start.3
  113.6 72.1 %all_to_all.20 = bf16[128,160,128]{2,1,0:T(8,128)(2,1)} all-to-all(bf16[128,160,128]{2,1,0:T(8,128)(2,1)S(1)} %bitcast.26), channel_id=1, replica_groups=mesh['sp'=16,'dp'=8] {'sp','dp'}, dimensions={0} | all-to-all | bytes 10485760 | tf_op jit(solution)/shard_map/all_to_all | solution.py:295
  185.7 0.0 copy-done.3
  185.7 31.4 %expert.1 = bf16[640,32,128]{2,1,0:T(8,128)(2,1)} custom-call(bf16[640,32,128]{2,1,0:T(8,128)(2,1)} %bitcast.31, bf16[1,4096,512]{2,1,0:T(8,128)(2,1)S(1)} %copy-done.3, bf16[1,4096,512]{2,1,0:T(8,128)(2,1)} %up_ref.1, bf16[1,512,4096]{2,1,0:T(8,128)(2,1)} %down_ref.1), custom_call_target="tpu_custom_call" | custom-call | flops 8000000000 | bytes 24000000 | tf_op jit(solution)/shard_map/expert/pallas_call | solution.py:299
  217.1 0.0 copy-start.7
  217.1 6.0 %all-to-all-start.3 = ((bf16[128,160,128]{2,1,0:T(8,128)(2,1)}), bf16[128,160,128]{2,1,0:T(8,128)(2,1)}, u32[]{:S(2)}, u32[]{:S(2)}) async-start(bf16[128,160,128]{2,1,0:T(8,128)(2,1)} %bitcast.30), calls=%async_computation.3 | async-start | bytes 10485760 | tf_op jit(solution)/shard_map/all_to_all | solution.py:318
  223.1 0.0 copy-done.7
  223.1 0.1 copy.25
  223.2 0.1 reshape.94.weight_ref
  223.3 63.9 %all-to-all-done.3 = bf16[128,160,128]{2,1,0:T(8,128)(2,1)} async-done(((bf16[128,160,128]{2,1,0:T(8,128)(2,1)}), bf16[128,160,128]{2,1,0:T(8,128)(2,1)}, u32[]{:S(2)}, u32[]{:S(2)}) %all-to-all-start.3) | async-done | bytes 5242912 | tf_op jit(solution)/shard_map/all_to_all | solution.py:318
  287.2 6.4 %combine.1 = bf16[128,4096]{1,0:T(8,128)(2,1)} custom-call(s32[512]{0:T(512)S(1)} %multiply_add_fusion.target_ref, f32[512]{0:T(512)S(1)} %reshape.94.weight_ref, bf16[640,32,128]{2,1,0:T(8,128)(2,1)} %bitcast.18.back_ref, bf16[128,32,128]{2,1,0:T(8,128)(2,1)S(1)} %get-tuple-element.8.hidden_ref), custom_call_target="tpu_custom_call" | custom-call | flops 400000000 | bytes 8000000 | tf_op jit(solution)/shard_map/combine/pallas_call | solution.py:319
  (8 shorter events, 0.1 us)
Async XLA Ops:
  6.5 36.7 %copy-start.6 = (s32[1,128,4]{1,2,0:T(4,128)S(1)}, s32[1,128,4]{1,2,0:T(4,128)}, u32[]{:S(2)}) copy-start(s32[1,128,4]{1,2,0:T(4,128)} %param.23) | copy-start | bytes 6148
  6.5 91.1 %all-gather.4.cloned.1.call-start = ((), (), s32[]{:S(2)}) async-start(), calls=%async_computation.4 | async-start | bytes 18874368 | tf_op jit(solution)/shard_map/all_gather | solution.py:211
  38.7 58.9 %copy-start = (bf16[1,128,4096]{2,1,0:T(8,128)(2,1)S(1)}, bf16[1,128,4096]{2,1,0:T(8,128)(2,1)}, u32[]{:S(2)}) copy-start(bf16[1,128,4096]{2,1,0:T(8,128)(2,1)} %param.20) | copy-start | bytes 3145732
  38.7 58.9 %copy-start.2 = (f32[4096]{0:T(1024)S(1)}, f32[4096]{0:T(1024)}, u32[]{:S(2)}) copy-start(f32[4096]{0:T(1024)} %param.22) | copy-start | bytes 49156
  38.7 13.8 %all-to-all-start = ((bf16[16,144,128]{2,1,0:T(8,128)(2,1)}), bf16[16,144,128]{2,1,0:T(8,128)(2,1)S(1)}, u32[]{:S(2)}, u32[]{:S(2)}) async-start(bf16[16,144,128]{2,1,0:T(8,128)(2,1)} %push.1), calls=%async_computation | async-start | bytes 1179648 | tf_op jit(solution)/shard_map/all_to_all | solution.py:232
  52.6 0.8 copy-start.4
  55.4 12.5 %all-to-all-start.1 = ((bf16[16,128,128]{2,1,0:T(8,128)(2,1)}), bf16[16,128,128]{2,1,0:T(8,128)(2,1)S(1)}, u32[]{:S(2)}, u32[]{:S(2)}) async-start(bf16[16,128,128]{2,1,0:T(8,128)(2,1)} %scan.1), calls=%async_computation.1 | async-start | bytes 1048576 | tf_op jit(solution)/shard_map/all_to_all | solution.py:239
  67.9 0.8 copy-start.5
  97.6 1.0 copy-start.1
  113.6 72.1 %copy-start.3 = (bf16[1,4096,512]{2,1,0:T(8,128)(2,1)S(1)}, bf16[1,4096,512]{2,1,0:T(8,128)(2,1)}, u32[]{:S(2)}) copy-start(bf16[1,4096,512]{2,1,0:T(8,128)(2,1)} %gate_ref.1) | copy-start | bytes 12582916
  217.1 6.0 %copy-start.7 = (f32[1,128,4]{1,2,0:T(4,128)S(1)}, f32[1,128,4]{1,2,0:T(4,128)}, u32[]{:S(2)}) copy-start(f32[1,128,4]{1,2,0:T(4,128)} %param.24) | copy-start | bytes 6148
  217.1 70.1 %all-to-all-start.3 = ((bf16[128,160,128]{2,1,0:T(8,128)(2,1)}), bf16[128,160,128]{2,1,0:T(8,128)(2,1)}, u32[]{:S(2)}, u32[]{:S(2)}) async-start(bf16[128,160,128]{2,1,0:T(8,128)(2,1)} %bitcast.30), calls=%async_computation.3 | async-start | bytes 10485760 | tf_op jit(solution)/shard_map/all_to_all | solution.py:318
Sparse Core Ops, SparseCore 0:
  9.0 88.5 all-gather.3

commit v2 on v1

v2 whole, which is shorter than its diff:
```python
import functools

import jax
import jax.numpy as jnp
from jax import lax
from jax.experimental import pallas as pl
from jax.experimental.pallas import tpu as pltpu
from jax.sharding import PartitionSpec as P

NORM_EPS = 1e-06
LANES = 128
CAPACITY = 5
BF16 = jnp.bfloat16
F32 = jnp.float32
MSG_PAD = 16


def dot(a, b, dims=((1,), (0,)), precision=None):
    return lax.dot_general(
        a, b, (dims, ((), ())), preferred_element_type=F32, precision=precision
    )


def split(x):
    high = x.astype(BF16)
    return high, (x - high.astype(F32)).astype(BF16)


def tril(rows):
    at = lax.broadcasted_iota(jnp.int32, (rows, rows), 0)
    of = lax.broadcasted_iota(jnp.int32, (rows, rows), 1)
    return of <= at


def gate_terms(forget, free):
    leak = free * jax.nn.sigmoid(-forget.astype(F32))
    causal = jnp.where(tril(leak.shape[0]), 1.0, 0.0)
    log_run = dot(causal, jnp.log1p(-leak), precision=lax.Precision.HIGHEST)
    return leak, log_run


def pair_kernel(forget_ref, value_ref, out_ref):
    size = out_ref.shape[3]
    for h in range(out_ref.shape[0]):
        out_ref[h, 0] = forget_ref[:, h * size : (h + 1) * size]
        out_ref[h, 1] = value_ref[:, h * size : (h + 1) * size]


def state_kernel(pair_ref, bound_ref, before_ref):
    blocks, _, rows, size = pair_ref.shape
    free = 1.0 - bound_ref[...]
    high = free.astype(BF16).astype(F32)
    mid = (free - high).astype(BF16).astype(F32)
    low = free - high - mid
    row = lax.broadcasted_iota(jnp.int32, (MSG_PAD, size), 0)
    tail = jnp.where(
        row == 0, high, jnp.where(row == 1, mid, jnp.where(row == 2, low, 0.0))
    ).astype(BF16)
    group = 4

    def some(i, state):
        forget = jnp.concatenate([pair_ref[i * group + j, 0] for j in range(group)], axis=1)
        leak, log_run = gate_terms(forget, jnp.concatenate([free] * group, axis=1))
        log_last = log_run[rows - 1 : rows, :]
        carry = leak * jnp.exp(log_last - log_run)
        keep = jnp.exp(log_last)
        for j in range(group):
            n = i * group + j
            before_ref[n, 0:size, :] = state.astype(BF16)
            before_ref[n, size : size + MSG_PAD, :] = tail
            at = slice(j * size, (j + 1) * size)
            upper, lower = split(carry[:, at])
            value = pair_ref[n, 1]
            push = dot(value, upper, ((0,), (0,))) + dot(value, lower, ((0,), (0,)))
            state = keep[:, at] * state + push
        return state

    lax.fori_loop(0, blocks // group, some, jnp.zeros((size, size), F32))


def mix_kernel(query_ref, forget_ref, value_ref, gate_ref, before_ref, gain_ref, out_ref):
    heads, _, size = before_ref.shape
    tails = [before_ref[h, size : size + MSG_PAD, :].astype(F32) for h in range(heads)]
    free = jnp.concatenate([t[2:3] + t[1:2] + t[0:1] for t in tails], axis=1)
    leak, log_run = gate_terms(forget_ref[...], free)
    q_scaled = query_ref[...].astype(F32) * jnp.exp(log_run)
    k_scaled = leak * jnp.exp(-log_run)
    q_high, q_low = split(q_scaled)
    k_high, k_low = split(k_scaled)
    causal = tril(leak.shape[0])
    u = gate_ref[...].astype(F32)
    silu = u / (1.0 + jnp.exp(-u))
    lanes = ((1,), (1,))
    for h in range(heads):
        at = slice(h * size, (h + 1) * size)
        scores = (
            dot(q_high[:, at], k_high[:, at], lanes)
            + dot(q_high[:, at], k_low[:, at], lanes)
            + dot(q_low[:, at], k_high[:, at], lanes)
        )
        s_high, s_low = split(jnp.where(causal, scores, 0.0))
        value = value_ref[:, at]
        before = before_ref[h, 0:size, :]
        mix = (
            dot(s_high, value)
            + dot(s_low, value)
            + dot(q_high[:, at], before, lanes)
            + dot(q_low[:, at], before, lanes)
        )
        scale = lax.rsqrt(jnp.mean(mix * mix, axis=-1, keepdims=True) + NORM_EPS)
        normed = (mix * scale * gain_ref[...]).astype(BF16)
        out_ref[:, at] = (normed.astype(F32) * silu[:, at]).astype(BF16)


def block_products(rows_ref, refs):
    at, total = 0, None
    for w_ref in refs:
        depth = w_ref.shape[0]
        part = dot(rows_ref[:, at : at + depth], w_ref[...])
        total = part if total is None else total + part
        at += depth
        if at == rows_ref.shape[1]:
            yield total.astype(BF16)
            at, total = 0, None


def columns_kernel(mine_ref, other_ref, *refs):
    *w_refs, keep_ref, give_ref = refs
    columns = w_refs[0].shape[1]
    for src, dst in ((mine_ref, keep_ref), (other_ref, give_ref)):
        for n, block in enumerate(block_products(src, w_refs)):
            dst[:, n * columns : (n + 1) * columns] = block


def route_kernel(slot_ref, order_ref, *refs):
    *part_refs, residual_ref, gain_ref, outgoing_ref, hidden_ref, wide_ref, moe_ref, keep_ref = refs
    tokens, width = residual_ref.shape
    pieces = width // LANES
    columns = width // order_ref.shape[0]
    skew = moe_ref.shape[0] // pieces
    squares = jnp.zeros((tokens, 1), F32)
    parts = [
        ref[:, n * columns : (n + 1) * columns]
        for ref in part_refs
        for n in range(ref.shape[1] // columns)
    ]
    for n, part in enumerate(parts):
        at = pl.multiple_of(order_ref[n] * columns, columns)
        hidden = residual_ref[:, pl.ds(at, columns)].astype(F32) + part.astype(F32)
        hidden = hidden.astype(BF16).astype(F32)
        wide_ref[:, pl.ds(at, columns)] = hidden
        squares = squares + jnp.sum(hidden * hidden, axis=-1, keepdims=True)
    scale = lax.rsqrt(squares / width + NORM_EPS)
    for c in range(pieces):
        part = wide_ref[:, c * LANES : (c + 1) * LANES]
        keep_ref[c * skew : c * skew + tokens, :] = part
        gain = gain_ref[:, c * LANES : (c + 1) * LANES]
        moe_ref[c * skew : c * skew + tokens, :] = part * scale * gain

    def keep_row(t, _):
        hidden_ref[t] = keep_ref[pl.ds(t, pieces, stride=skew), :].astype(BF16)
        return 0

    lax.fori_loop(0, tokens, keep_row, 0, unroll=4)

    def fill_slot(s, _):
        outgoing_ref[s] = moe_ref[pl.ds(slot_ref[s], pieces, stride=skew), :].astype(BF16)
        return 0

    lax.fori_loop(0, outgoing_ref.shape[0], fill_slot, 0, unroll=8)


def expert_kernel(rows_ref, gate_ref, up_ref, down_ref, out_ref, wide_ref, x_ref):
    pieces = rows_ref.shape[1]
    rows = x_ref.shape[0]
    skew = wide_ref.shape[0] // pieces

    def some(i, _):
        first = i * rows

        def spread(r, _):
            wide_ref[pl.ds(r, pieces, stride=skew), :] = rows_ref[first + r].astype(F32)
            return 0

        lax.fori_loop(0, rows, spread, 0, unroll=8)
        for c in range(pieces):
            x_ref[:, c * LANES : (c + 1) * LANES] = wide_ref[
                c * skew : c * skew + rows, :
            ].astype(BF16)
        gate = dot(x_ref[...], gate_ref[...])
        up = dot(x_ref[...], up_ref[...])
        act = (gate / (1.0 + jnp.exp(-gate)) * up).astype(BF16)
        step = 4
        for c in range(0, pieces, step):
            part = dot(act, down_ref[:, c * LANES : (c + step) * LANES])
            for k in range(step):
                wide_ref[(c + k) * skew : (c + k) * skew + rows, :] = part[
                    :, k * LANES : (k + 1) * LANES
                ]

        def gather(r, _):
            out_ref[first + r] = wide_ref[pl.ds(r, pieces, stride=skew), :].astype(BF16)
            return 0

        lax.fori_loop(0, rows, gather, 0, unroll=8)
        return 0

    lax.fori_loop(0, rows_ref.shape[0] // rows, some, 0)


def combine_kernel(target_ref, weight_ref, back_ref, hidden_ref, out_ref, wide_ref):
    tokens, pieces, _ = hidden_ref.shape
    skew = wide_ref.shape[0] // pieces
    top = target_ref.shape[0] // tokens

    def one(t, _):
        total = jnp.zeros((pieces, LANES), F32)
        for j in range(top):
            i = t * top + j
            total = total + weight_ref[i] * back_ref[target_ref[i]].astype(F32)
        wide_ref[pl.ds(t, pieces, stride=skew), :] = hidden_ref[t].astype(F32) + total
        return 0

    lax.fori_loop(0, tokens, one, 0, unroll=4)
    for c in range(pieces):
        out_ref[:, c * LANES : (c + 1) * LANES] = wide_ref[
            c * skew : c * skew + tokens, :
        ].astype(BF16)


def whole(shape, space=None):
    if space is None:
        return pl.BlockSpec(shape, lambda *_: (0,) * len(shape))
    return pl.BlockSpec(memory_space=space)


def cost(flops, moved):
    return pl.CostEstimate(flops=int(flops), bytes_accessed=int(moved), transcendentals=0)


def slots_of(chosen, experts, capacity, tokens, top_count):
    matches = (chosen[:, None] == jnp.arange(experts, dtype=jnp.int32)[None, :]).astype(jnp.int32)
    rank_in = jnp.sum((jnp.cumsum(matches, axis=0) - 1) * matches, axis=1)
    target = chosen * capacity + rank_in
    owners = jnp.arange(tokens * top_count, dtype=jnp.int32) // top_count
    slot_owner = jnp.zeros((experts * capacity,), jnp.int32).at[target].set(owners)
    return target, slot_owner


def local(
    queries,
    forget_pre,
    values,
    out_gate,
    lower_bound,
    head_gain,
    residual,
    out_weight,
    ffn_gain,
    routing,
    route_weight,
    expert_gate,
    expert_up,
    expert_down,
):
    tokens = queries.shape[1]
    channels = queries.shape[2]
    size = head_gain.shape[0]
    heads = channels // size
    width = residual.shape[2]
    pieces = width // LANES
    top_count = routing.shape[2]
    span = lax.axis_size("sp") * lax.axis_size("dp")
    experts = expert_gate.shape[0] * span
    slots = experts * CAPACITY

    half = channels // 2
    upper, lower = out_weight[:half], out_weight[half:]
    ring = lax.axis_size("dp")
    forward = [(d, (d + 2) % ring) for d in range(ring)]
    backward = [(d, (d + ring - 2) % ring) for d in range(ring)]
    across = [(d, d ^ 1) for d in range(ring)]
    before_upper = lax.ppermute(upper, "dp", forward)
    after_lower = lax.ppermute(lower, "dp", backward)
    before_lower = lax.ppermute(lower, "dp", forward)
    after_upper = lax.ppermute(upper, "dp", backward)

    def swap(x):
        return lax.ppermute(x, "dp", across)

    in_vmem = whole(None, pltpu.VMEM)
    q = queries.reshape(tokens, channels)
    f = forget_pre.reshape(tokens, channels)
    v = values.reshape(tokens, channels)
    g = out_gate.reshape(tokens, channels)
    pair = pl.pallas_call(
        pair_kernel,
        in_specs=[in_vmem, in_vmem],
        out_specs=in_vmem,
        out_shape=jax.ShapeDtypeStruct((heads, 2, tokens, size), BF16),
        cost_estimate=cost(1e6, 2e6),
        compiler_params=pltpu.CompilerParams(vmem_limit_bytes=8 * 2**20),
        name="pair",
    )(f, v)
    arrived = lax.all_to_all(pair, "sp", split_axis=0, concat_axis=0, tiled=True)
    arrived, before_upper, after_lower = lax.optimization_barrier(
        (arrived, before_upper, after_lower)
    )
    far_upper = lax.ppermute(before_upper, "dp", forward)
    far_lower = lax.ppermute(after_lower, "dp", backward)
    before = pl.pallas_call(
        state_kernel,
        in_specs=[in_vmem, in_vmem],
        out_specs=in_vmem,
        out_shape=jax.ShapeDtypeStruct((arrived.shape[0], size + MSG_PAD, size), BF16),
        cost_estimate=cost(1e9, 2e6),
        compiler_params=pltpu.CompilerParams(vmem_limit_bytes=12 * 2**20),
        name="state",
    )(arrived, lower_bound.reshape(1, size))
    before = lax.all_to_all(before, "sp", split_axis=0, concat_axis=0, tiled=True)
    before, before_lower, after_upper = lax.optimization_barrier(
        (before, before_lower, after_upper)
    )
    target, slot_owner = slots_of(
        routing.reshape(tokens * top_count), experts, CAPACITY, tokens, top_count
    )
    per_step = 4
    head_block = pl.BlockSpec((tokens, per_step * size), lambda h: (0, h))
    gated = pl.pallas_call(
        mix_kernel,
        grid=(heads // per_step,),
        in_specs=[head_block] * 4
        + [
            pl.BlockSpec((per_step, size + MSG_PAD, size), lambda h: (h, 0, 0)),
            pl.BlockSpec((1, size), lambda h: (0, 0)),
        ],
        out_specs=head_block,
        out_shape=jax.ShapeDtypeStruct((tokens, channels), BF16),
        cost_estimate=cost(2e9, 3e6),
        compiler_params=pltpu.CompilerParams(vmem_limit_bytes=60 * 2**20),
        name="mix",
    )(q, f, v, g, before, head_gain.reshape(1, size))

    gated, slot_owner, target = lax.optimization_barrier((gated, slot_owner, target))
    gated_other = swap(gated)
    columns = out_weight.shape[1]

    def project(limit, *parts):
        wide = sum(p.shape[0] for p in parts) // channels * columns
        shape = jax.ShapeDtypeStruct((tokens, wide), BF16)
        keep, give = pl.pallas_call(
            columns_kernel,
            in_specs=[in_vmem] * (2 + len(parts)),
            out_specs=[in_vmem] * 2,
            out_shape=[shape] * 2,
            cost_estimate=cost(4 * tokens * channels * wide, 2 * channels * wide),
            compiler_params=pltpu.CompilerParams(vmem_limit_bytes=limit * 2**20),
        )(gated, gated_other, *parts)
        return keep, swap(give)

    near = project(14, out_weight, before_upper, before_lower, after_upper, after_lower)
    near, far_upper, far_lower = lax.optimization_barrier((near, far_upper, far_lower))
    far = project(8, far_upper, far_lower)
    chip, core = lax.axis_index("dp") // 2, lax.axis_index("dp") % 2
    order = jnp.stack(
        [
            (chip + hop) % (ring // 2) * 2 + parity
            for hops in ((0, ring // 2 - 1, 1), (2,))
            for parity in (core, 1 - core)
            for hop in hops
        ]
    ).astype(jnp.int32)
    skew = tokens + 1
    outgoing, hidden = pl.pallas_call(
        route_kernel,
        in_specs=[whole(None, pltpu.SMEM)] * 2 + [in_vmem] * 6,
        out_specs=[in_vmem, in_vmem],
        out_shape=[
            jax.ShapeDtypeStruct((slots, pieces, LANES), BF16),
            jax.ShapeDtypeStruct((tokens, pieces, LANES), BF16),
        ],
        scratch_shapes=[
            pltpu.VMEM((tokens, width), F32),
            pltpu.VMEM((skew * pieces, LANES), F32),
            pltpu.VMEM((skew * pieces, LANES), F32),
        ],
        cost_estimate=cost(4e7, 12e6),
        compiler_params=pltpu.CompilerParams(vmem_limit_bytes=24 * 2**20),
        name="route",
    )(
        slot_owner,
        order,
        *near,
        *far,
        residual.reshape(tokens, width),
        ffn_gain.reshape(1, width),
    )

    exchange = functools.partial(
        lax.all_to_all, axis_name=("sp", "dp"), split_axis=0, concat_axis=0, tiled=True
    )
    chunk = (span, CAPACITY * pieces, LANES)
    rows_in = exchange(outgoing.reshape(chunk)).reshape(slots, pieces, LANES)
    hidden_units = expert_gate.shape[2]
    rows = slots // 2
    results = pl.pallas_call(
        expert_kernel,
        in_specs=[in_vmem] * 4,
        out_specs=in_vmem,
        out_shape=jax.ShapeDtypeStruct((slots, pieces, LANES), BF16),
        scratch_shapes=[
            pltpu.VMEM(((rows + 1) * pieces, LANES), F32),
            pltpu.VMEM((rows, width), BF16),
        ],
        cost_estimate=cost(8e9, 24e6),
        compiler_params=pltpu.CompilerParams(vmem_limit_bytes=34 * 2**20),
        name="expert",
    )(
        rows_in,
        expert_gate.reshape(width, hidden_units),
        expert_up.reshape(width, hidden_units),
        expert_down.reshape(hidden_units, width),
    )
    back = exchange(results.reshape(chunk)).reshape(slots, pieces, LANES)
    out = pl.pallas_call(
        combine_kernel,
        in_specs=[
            whole(None, pltpu.SMEM),
            whole(None, pltpu.SMEM),
            whole(None, pltpu.VMEM),
            whole(None, pltpu.VMEM),
        ],
        out_specs=whole(None, pltpu.VMEM),
        out_shape=jax.ShapeDtypeStruct((tokens, width), BF16),
        scratch_shapes=[pltpu.VMEM((skew * pieces, LANES), F32)],
        cost_estimate=cost(4e8, 8e6),
        compiler_params=pltpu.CompilerParams(vmem_limit_bytes=16 * 2**20),
        name="combine",
    )(target, route_weight.reshape(tokens * top_count), back, hidden)
    return out.reshape(1, tokens, width)


def solution(mesh):
    in_specs = (
        P("dp", "sp", None),
        P("dp", "sp", None),
        P("dp", "sp", None),
        P("dp", "sp", None),
        P("sp"),
        P(),
        P("dp", "sp", None),
        P(None, "dp"),
        P(),
        P("dp", "sp", None),
        P("dp", "sp", None),
        P(("sp", "dp"), None, None),
        P(("sp", "dp"), None, None),
        P(("sp", "dp"), None, None),
    )
    out_specs = P("dp", "sp", None)
    return jax.shard_map(local, mesh=mesh, in_specs=in_specs, out_specs=out_specs, check_vma=False)
```

time: 304 us -> 281 us (0.924); the launches traced: 300 us -> 281 us
  Pallas kernels: 78.9 us -> 36.5 us
  waiting for transfers between devices: 94.8 us -> 122 us
  blocking collectives: 92.6 us -> 68.8 us
  starting transfers between devices: 14 us -> 34.6 us
  between operations: 13.5 us -> 0.2 us
  local copies, waits for them, and re-layouts: 6.02 us -> 16.4 us
    pallas_call x5 -> x7, Pallas kernels: 72.5 us -> 31.6 us  [the longest x1 13 us: local(): pl.pallas_call(expert_kernel, in_specs=[in_vmem] * 4, out_specs=in_vmem,...]
    ppermute x0 -> x9, waiting for transfers between devices: none -> 39 us  [the longest x1 20.9 us: local(): before_upper = lax.ppermute(upper, 'dp', forward)]
    all_gather x1 -> x0, blocking collectives: 20.6 us -> none  [local(): bound = lax.all_gather(lower_bound, 'sp', tiled=True).reshape(1, channels)]
    all_gather x1 -> x0, waiting for transfers between devices: 15.6 us -> none  [local(): weights_all = lax.all_gather(out_weight, 'dp')]
    ppermute x0 -> x9, starting transfers between devices: none -> 13.2 us  [the longest x3 4.31 us: swap(): return lax.ppermute(x, 'dp', across)]
    unnamed x18 -> x38, local copies, waits for them, and re-layouts: 2.9 us -> 8.61 us
    all_to_all x1, starting transfers between devices: 3.57 us -> 7.78 us  [local(): lax.all_to_all(before, 'sp', split_axis=0, concat_axis=0, tiled=True)]
    all_to_all x1, waiting for transfers between devices: 8.67 us -> 12.3 us  [local(): lax.all_to_all(pair, 'sp', split_axis=0, concat_axis=0, tiled=True)]
  transfers between devices with their start and end apart: 4 -> 12, of which waited for: 4 -> 6; matrix products, arithmetic and copies ran while one was open for 1% -> 2% of each run, Pallas kernels for 9% -> 3%
where the time goes in v2:
time: 281 us
  waiting for transfers between devices  122 us (43%)
  blocking collectives  68.8 us (24%)
  Pallas kernels  36.5 us (13%)
  starting transfers between devices  34.6 us (12%)
  local copies, waits for them, and re-layouts  16.4 us (6%)
    all_to_all x1, blocking collectives, local(): rows_in = exchange(outgoing.reshape(chunk)).reshape(slots, pieces, LANES)  68.8 us
    all_to_all x1, waiting for transfers between devices, local(): back = exchange(results.reshape(chunk)).reshape(slots, pieces, LANES)  63.9 us
    ppermute x1, waiting for transfers between devices, local(): before_upper = lax.ppermute(upper, 'dp', forward)  20.9 us
    ppermute x1, waiting for transfers between devices, local(): far_upper = lax.ppermute(before_upper, 'dp', forward)  17.2 us
    pallas_call x1, Pallas kernels, local(): pl.pallas_call(expert_kernel, in_specs=[in_vmem] * 4, out_specs=in_vmem,...  13 us
    all_to_all x1, waiting for transfers between devices, local(): lax.all_to_all(pair, 'sp', split_axis=0, concat_axis=0, tiled=True)  12.3 us
    unnamed x38, local copies, waits for them, and re-layouts  8.61 us
    all_to_all x1, starting transfers between devices, local(): lax.all_to_all(before, 'sp', split_axis=0, concat_axis=0, tiled=True)  7.78 us
  transfers between devices with their start and end apart: 12, of which 6 were waited for; matrix products, arithmetic and copies ran while one was open for 2% of the time, Pallas kernels for 3%

profile of v2, /device:TPU:1, one launch (start us, length us, event | category | flops | bytes accessed | tf_op | source)
XLA Modules:
  0.0 280.6 jit_solution(13528483348042586225)
XLA Ops:
  0.0 3.1 %fusion.9 = (bf16[1024,512]{1,0:T(8,128)(2,1)}, bf16[1024,512]{1,0:T(8,128)(2,1)}) fusion(bf16[2048,512]{1,0:T(8,128)(2,1)} %refs_0_.1), kind=kLoop, calls=%fused_computation.22 | loop fusion | bytes 4194304 | tf_op jit(solution)/shard_map/slice | solution.py:278
  3.1 3.6 %collective-permute-start.1 = (bf16[1024,512]{1,0:T(8,128)(2,1)}, bf16[1024,512]{1,0:T(8,128)(2,1)S(1)}, u32[]{:S(2)}, u32[]{:S(2)}) collective-permute-start(bf16[1024,512]{1,0:T(8,128)(2,1)} %get-tuple-element.43), channel_id=1, source_target_pairs={{0,6},{1,7},{2,0},{3,1},{4,2},{5,3},{6,4},{7,5},{8,14},{9,15},{10,... | collective-permute-start | bytes 3145736 | tf_op jit(solution)/shard_map/ppermute | solution.py:284
  6.6 0.0 collective-permute-start
  6.7 2.7 collective-permute-start.3
  9.3 1.2 pair.1
  10.5 7.6 %all-to-all-start = ((bf16[16,2,128,128]{3,2,1,0:T(8,128)(2,1)}), bf16[16,2,128,128]{3,2,1,0:T(8,128)(2,1)S(1)}, u32[]{:S(2)}, u32[]{:S(2)}) async-start(bf16[16,2,128,128]{3,2,1,0:T(8,128)(2,1)} %pair.1), calls=%async_computation | async-start | bytes 2097152 | tf_op jit(solution)/shard_map/all_to_all | solution.py:305
  18.1 0.1 copy.16
  18.2 0.1 eq.39
  18.3 0.1 copy.18
  18.4 0.2 fusion.1
  18.7 0.8 add_add_fusion
  19.5 0.1 eq.35
  19.6 1.0 copy.19
  20.6 0.1 copy.15
  20.7 0.1 mul.41
  20.8 0.2 fusion
  21.0 12.3 %all-to-all-done.pair_ref = bf16[16,2,128,128]{3,2,1,0:T(8,128)(2,1)S(1)} async-done(((bf16[16,2,128,128]{3,2,1,0:T(8,128)(2,1)}), bf16[16,2,128,128]{3,2,1,0:T(8,128)(2,1)S(1)}, u32[]{:S(2)}, u32[]{:S(2)}) %all-to-all-start) | async-done | bytes 1048608 | tf_op jit(solution)/shard_map/all_to_all | solution.py:305
  33.4 20.9 %collective-permute-done.refs_1_ = bf16[1024,512]{1,0:T(8,128)(2,1)S(1)} collective-permute-done((bf16[1024,512]{1,0:T(8,128)(2,1)}, bf16[1024,512]{1,0:T(8,128)(2,1)S(1)}, u32[]{:S(2)}, u32[]{:S(2)}) %collective-permute-start) | collective-permute-done | bytes 1048608 | tf_op jit(solution)/shard_map/ppermute | solution.py:283
  54.3 1.0 copy-done.3
  55.3 3.0 %state.1 = bf16[16,144,128]{2,1,0:T(8,128)(2,1)S(1)} custom-call(bf16[16,2,128,128]{3,2,1,0:T(8,128)(2,1)S(1)} %all-to-all-done.pair_ref, f32[1,128]{1,0:T(1,128)S(1)} %bitcast.45), custom_call_target="tpu_custom_call" | custom-call | flops 1000000000 | bytes 2000000 | tf_op jit(solution)/shard_map/state/pallas_call | solution.py:311
  58.2 0.8 copy-done.6
  59.1 7.8 %all-to-all-start.1 = ((bf16[16,144,128]{2,1,0:T(8,128)(2,1)}), bf16[16,144,128]{2,1,0:T(8,128)(2,1)}, u32[]{:S(2)}, u32[]{:S(2)}) async-start(bf16[16,144,128]{2,1,0:T(8,128)(2,1)} %copy-done.6), calls=%async_computation.1 | async-start | bytes 1179648 | tf_op jit(solution)/shard_map/all_to_all | solution.py:320
  66.9 3.0 %scatter_custom_fusion.slot_ref = s32[640]{0:T(1024)} fusion(s32[512]{0:T(512)S(1)} %bitcast.48, s32[512]{0:T(512)S(1)} %add_select_fusion, s32[]{:T(128)} %constant.76.clone.1), kind=kCustom, calls=%fused_computation.18 | custom fusion | bytes 2564 | tf_op jit(solution)/shard_map/scatter | solution.py:246
  69.9 0.6 multiply_add_fusion.target_ref
  70.5 6.9 %all-to-all-done.1.before_ref = bf16[16,144,128]{2,1,0:T(8,128)(2,1)} async-done(((bf16[16,144,128]{2,1,0:T(8,128)(2,1)}), bf16[16,144,128]{2,1,0:T(8,128)(2,1)}, u32[]{:S(2)}, u32[]{:S(2)}) %all-to-all-start.1) | async-done | bytes 589856 | tf_op jit(solution)/shard_map/all_to_all | solution.py:320
  77.4 7.5 %mix.1.mine_ref = bf16[128,2048]{1,0:T(8,128)(2,1)} custom-call(bf16[128,2048]{1,0:T(8,128)(2,1)} %bitcast.49, bf16[128,2048]{1,0:T(8,128)(2,1)} %bitcast.37, bf16[128,2048]{1,0:T(8,128)(2,1)} %bitcast.39, bf16[128,2048]{1,0:T(8,128)(2,1)} %bitcast.50, bf16[16,144,128]{2,1,0:T(8,128)(2,1)} %all-to-all-done.1.before_ref, f32[1,128]{1,0:T(1,128)} %bitcast.51), custom_call_target="tpu_custom_call" | custom-call | flops 2000000000 | bytes 3000000 | tf_op jit(solution)/shard_map/mix/pallas_call | solution.py:329
  84.9 2.7 collective-permute-start.4
  87.6 2.7 collective-permute-start.7
  90.3 1.0 copy-done.2
  91.3 1.2 copy-done.4
  92.6 3.3 %shard_map.136 = (bf16[128,1536]{1,0:T(8,128)(2,1)S(1)}, bf16[128,1536]{1,0:T(8,128)(2,1)S(1)}) custom-call(bf16[128,2048]{1,0:T(8,128)(2,1)S(1)} %copy-done.2, bf16[128,2048]{1,0:T(8,128)(2,1)S(1)} %collective-permute-done.4.other_ref, bf16[2048,512]{1,0:T(8,128)(2,1)S(1)} %copy-done, bf16[1024,512]{1,0:T(8,128)(2,1)S(1)} %copy-done.4, ...), custom_call_target="tpu_custom_call" | custom-call | flops 1610612736 | bytes 6291456 | tf_op jit(solution)/shard_map/pallas_call | solution.py:351
  95.9 0.6 collective-permute-start.5
  96.6 17.2 %collective-permute-done.6.refs_0_ = bf16[1024,512]{1,0:T(8,128)(2,1)S(1)} collective-permute-done((bf16[1024,512]{1,0:T(8,128)(2,1)}, bf16[1024,512]{1,0:T(8,128)(2,1)S(1)}, u32[]{:S(2)}, u32[]{:S(2)}) %collective-permute-start.6) | collective-permute-done | bytes 1048608 | tf_op jit(solution)/shard_map/ppermute | solution.py:309
  113.8 0.7 shard_map.137
  114.5 0.9 collective-permute-start.8
  115.4 0.1 stack.35.order_ref
  115.5 0.9 collective-permute-done.8.refs_3_
  116.4 1.2 copy-done.5
  117.6 0.7 copy-done.10
  118.3 2.9 %route.1 = (bf16[640,32,128]{2,1,0:T(8,128)(2,1)S(1)}, bf16[128,32,128]{2,1,0:T(8,128)(2,1)S(1)}) custom-call(s32[640]{0:T(1024)S(1)} %copy-done.10, s32[8]{0:T(128)S(1)} %stack.35.order_ref, bf16[128,1536]{1,0:T(8,128)(2,1)S(1)} %get-tuple-element.35.refs_0_, bf16[128,1536]{1,0:T(8,128)(2,1)S(1)} %collective-permute-done.5.refs_1_, ...), custom_call_target="tpu_custom_call" | custom-call | flops 40000000 | bytes 12000000 | tf_op jit(solution)/shard_map/route/pallas_call | solution.py:374
  121.2 68.8 %all_to_all.20 = bf16[128,160,128]{2,1,0:T(8,128)(2,1)} all-to-all(bf16[128,160,128]{2,1,0:T(8,128)(2,1)S(1)} %bitcast.34), channel_id=1, replica_groups=mesh['sp'=16,'dp'=8] {'sp','dp'}, dimensions={0} | all-to-all | bytes 10485760 | tf_op jit(solution)/shard_map/all_to_all | solution.py:403
  190.1 13.0 %expert.1 = bf16[640,32,128]{2,1,0:T(8,128)(2,1)S(1)} custom-call(bf16[640,32,128]{2,1,0:T(8,128)(2,1)} %bitcast.46, bf16[4096,512]{1,0:T(8,128)(2,1)S(1)} %bitcast.42, bf16[4096,512]{1,0:T(8,128)(2,1)S(1)} %bitcast.43, bf16[512,4096]{1,0:T(8,128)(2,1)S(1)} %bitcast.44), custom_call_target="tpu_custom_call" | custom-call | flops 8000000000 | bytes 24000000 | tf_op jit(solution)/shard_map/expert/pallas_call | solution.py:406
  203.1 2.4 copy-done.1
  205.5 6.0 %all-to-all-start.3 = ((bf16[128,160,128]{2,1,0:T(8,128)(2,1)}), bf16[128,160,128]{2,1,0:T(8,128)(2,1)}, u32[]{:S(2)}, u32[]{:S(2)}) async-start(bf16[128,160,128]{2,1,0:T(8,128)(2,1)} %bitcast.35), calls=%async_computation.3 | async-start | bytes 10485760 | tf_op jit(solution)/shard_map/all_to_all | solution.py:424
  211.5 0.1 copy.20
  211.6 0.1 reshape.106.weight_ref
  211.7 63.9 %all-to-all-done.3 = bf16[128,160,128]{2,1,0:T(8,128)(2,1)} async-done(((bf16[128,160,128]{2,1,0:T(8,128)(2,1)}), bf16[128,160,128]{2,1,0:T(8,128)(2,1)}, u32[]{:S(2)}, u32[]{:S(2)}) %all-to-all-start.3) | async-done | bytes 5242912 | tf_op jit(solution)/shard_map/all_to_all | solution.py:424
  275.7 4.9 %combine.1 = bf16[128,4096]{1,0:T(8,128)(2,1)} custom-call(s32[512]{0:T(512)S(1)} %copy-done.11, f32[512]{0:T(512)S(1)} %reshape.106.weight_ref, bf16[640,32,128]{2,1,0:T(8,128)(2,1)} %bitcast.27.back_ref, bf16[128,32,128]{2,1,0:T(8,128)(2,1)S(1)} %get-tuple-element.42.hidden_ref), custom_call_target="tpu_custom_call" | custom-call | flops 400000000 | bytes 8000000 | tf_op jit(solution)/shard_map/combine/pallas_call | solution.py:425
  (43 shorter events, 0.1 us)
Async XLA Ops:
  0.0 9.3 %copy-start.7 = (bf16[1,128,2048]{2,1,0:T(8,128)(2,1)S(1)}, bf16[1,128,2048]{2,1,0:T(8,128)(2,1)}, u32[]{:S(2)}) copy-start(bf16[1,128,2048]{2,1,0:T(8,128)(2,1)} %param.15) | copy-start | bytes 1572868
  0.0 9.3 %copy-start.8 = (bf16[1,128,2048]{2,1,0:T(8,128)(2,1)S(1)}, bf16[1,128,2048]{2,1,0:T(8,128)(2,1)}, u32[]{:S(2)}) copy-start(bf16[1,128,2048]{2,1,0:T(8,128)(2,1)} %param.16) | copy-start | bytes 1572868
  0.0 18.1 %copy-start.16 = (s32[1,128,4]{1,2,0:T(4,128)S(1)}, s32[1,128,4]{1,2,0:T(4,128)}, u32[]{:S(2)}) copy-start(s32[1,128,4]{1,2,0:T(4,128)} %param.23) | copy-start | bytes 6148
  0.0 55.3 %copy-start.15 = (f32[128]{0:T(128)S(1)}, f32[128]{0:T(128)}, u32[]{:S(2)}) copy-start(f32[128]{0:T(128)} %param.18) | copy-start | bytes 1540
  3.1 51.2 %collective-permute-start.1 = (bf16[1024,512]{1,0:T(8,128)(2,1)}, bf16[1024,512]{1,0:T(8,128)(2,1)S(1)}, u32[]{:S(2)}, u32[]{:S(2)}) collective-permute-start(bf16[1024,512]{1,0:T(8,128)(2,1)} %get-tuple-element.43), channel_id=1, source_target_pairs={{0,6},{1,7},{2,0},{3,1},{4,2},{5,3},{6,4},{7,5},{8,14},{9,15},{10,... | collective-permute-start | bytes 3145736 | tf_op jit(solution)/shard_map/ppermute | solution.py:284
  6.6 63.9 %collective-permute-start.2 = (bf16[1024,512]{1,0:T(8,128)(2,1)}, bf16[1024,512]{1,0:T(8,128)(2,1)}, u32[]{:S(2)}, u32[]{:S(2)}) collective-permute-start(bf16[1024,512]{1,0:T(8,128)(2,1)} %get-tuple-element.43), channel_id=1, source_target_pairs={{0,2},{1,3},{2,4},{3,5},{4,6},{5,7},{6,0},{7,1},{8,10},{9,11},{10,... | collective-permute-start | bytes 3145736 | tf_op jit(solution)/shard_map/ppermute | solution.py:285
  6.6 47.7 %collective-permute-start = (bf16[1024,512]{1,0:T(8,128)(2,1)}, bf16[1024,512]{1,0:T(8,128)(2,1)S(1)}, u32[]{:S(2)}, u32[]{:S(2)}) collective-permute-start(bf16[1024,512]{1,0:T(8,128)(2,1)} %get-tuple-element.44), channel_id=1, source_target_pairs={{0,2},{1,3},{2,4},{3,5},{4,6},{5,7},{6,0},{7,1},{8,10},{9,11},{10,... | collective-permute-start | bytes 3145736 | tf_op jit(solution)/shard_map/ppermute | solution.py:283
  6.7 63.8 %collective-permute-start.3 = (bf16[1024,512]{1,0:T(8,128)(2,1)}, bf16[1024,512]{1,0:T(8,128)(2,1)}, u32[]{:S(2)}, u32[]{:S(2)}) collective-permute-start(bf16[1024,512]{1,0:T(8,128)(2,1)} %get-tuple-element.44), channel_id=1, source_target_pairs={{0,6},{1,7},{2,0},{3,1},{4,2},{5,3},{6,4},{7,5},{8,14},{9,15},{10,... | collective-permute-start | bytes 3145736 | tf_op jit(solution)/shard_map/ppermute | solution.py:286
  10.5 22.9 %all-to-all-start = ((bf16[16,2,128,128]{3,2,1,0:T(8,128)(2,1)}), bf16[16,2,128,128]{3,2,1,0:T(8,128)(2,1)S(1)}, u32[]{:S(2)}, u32[]{:S(2)}) async-start(bf16[16,2,128,128]{3,2,1,0:T(8,128)(2,1)} %pair.1), calls=%async_computation | async-start | bytes 2097152 | tf_op jit(solution)/shard_map/all_to_all | solution.py:305
  54.3 1.0 copy-start.3
  58.2 0.8 copy-start.6
  59.1 31.2 %copy-start = (bf16[2048,512]{1,0:T(8,128)(2,1)S(1)}, bf16[2048,512]{1,0:T(8,128)(2,1)}, u32[]{:S(2)}) copy-start(bf16[2048,512]{1,0:T(8,128)(2,1)} %refs_0_.1) | copy-start | bytes 6291460
  59.1 18.4 %all-to-all-start.1 = ((bf16[16,144,128]{2,1,0:T(8,128)(2,1)}), bf16[16,144,128]{2,1,0:T(8,128)(2,1)}, u32[]{:S(2)}, u32[]{:S(2)}) async-start(bf16[16,144,128]{2,1,0:T(8,128)(2,1)} %copy-done.6), calls=%async_computation.1 | async-start | bytes 1179648 | tf_op jit(solution)/shard_map/all_to_all | solution.py:320
  77.4 39.0 %copy-start.9 = (f32[4096]{0:T(1024)S(1)}, f32[4096]{0:T(1024)}, u32[]{:S(2)}) copy-start(f32[4096]{0:T(1024)} %param.22) | copy-start | bytes 49156
  84.9 5.4 %collective-permute-start.4 = (bf16[128,2048]{1,0:T(8,128)(2,1)}, bf16[128,2048]{1,0:T(8,128)(2,1)S(1)}, u32[]{:S(2)}, u32[]{:S(2)}) collective-permute-start(bf16[128,2048]{1,0:T(8,128)(2,1)} %mix.1.mine_ref), channel_id=1, source_target_pairs={{0,1},{1,0},{2,3},{3,2},{4,5},{5,4},{6,7},{7,6},{8,9},{9,8},{10,11... | collective-permute-start | bytes 1572872 | tf_op jit(solution)/shard_map/ppermute | solution.py:289
  87.6 26.1 %collective-permute-start.6 = (bf16[1024,512]{1,0:T(8,128)(2,1)}, bf16[1024,512]{1,0:T(8,128)(2,1)S(1)}, u32[]{:S(2)}, u32[]{:S(2)}) collective-permute-start(bf16[1024,512]{1,0:T(8,128)(2,1)} %copy-done.3), channel_id=1, source_target_pairs={{0,2},{1,3},{2,4},{3,5},{4,6},{5,7},{6,0},{7,1},{8,10},{9,11},{10,... | collective-permute-start | bytes 3145736 | tf_op jit(solution)/shard_map/ppermute | solution.py:309
  87.6 26.1 %collective-permute-start.7 = (bf16[1024,512]{1,0:T(8,128)(2,1)S(1)}, bf16[1024,512]{1,0:T(8,128)(2,1)S(1)}, u32[]{:S(2)}, u32[]{:S(2)}) collective-permute-start(bf16[1024,512]{1,0:T(8,128)(2,1)S(1)} %collective-permute-done.1.refs_4_), channel_id=1, source_target_pairs={{0,6},{1,7},{2,0},{3,1},{4,2},{5,3},{6,4},{7,5},{8,14},{9,15},{10,... | collective-permute-start | bytes 3145736 | tf_op jit(solution)/shard_map/ppermute | solution.py:310
  90.3 1.0 copy-start.2
  91.3 1.2 copy-start.4
  95.9 17.8 %collective-permute-start.5 = (bf16[128,1536]{1,0:T(8,128)(2,1)S(1)}, bf16[128,1536]{1,0:T(8,128)(2,1)S(1)}, u32[]{:S(2)}, u32[]{:S(2)}) collective-permute-start(bf16[128,1536]{1,0:T(8,128)(2,1)S(1)} %get-tuple-element.34), channel_id=1, source_target_pairs={{0,1},{1,0},{2,3},{3,2},{4,5},{5,4},{6,7},{7,6},{8,9},{9,8},{10,11... | collective-permute-start | bytes 1179656 | tf_op jit(solution)/shard_map/ppermute | solution.py:289
  114.5 1.9 collective-permute-start.8
  116.4 1.2 copy-start.5
  117.6 0.7 copy-start.10
  118.3 71.7 %copy-start.14 = (bf16[1,512,4096]{2,1,0:T(8,128)(2,1)S(1)}, bf16[1,512,4096]{2,1,0:T(8,128)(2,1)}, u32[]{:S(2)}) copy-start(bf16[1,512,4096]{2,1,0:T(8,128)(2,1)} %param.27) | copy-start | bytes 12582916
  121.2 68.8 %copy-start.12 = (bf16[1,4096,512]{2,1,0:T(8,128)(2,1)S(1)}, bf16[1,4096,512]{2,1,0:T(8,128)(2,1)}, u32[]{:S(2)}) copy-start(bf16[1,4096,512]{2,1,0:T(8,128)(2,1)} %param.25) | copy-start | bytes 12582916
  121.2 68.8 %copy-start.13 = (bf16[1,4096,512]{2,1,0:T(8,128)(2,1)S(1)}, bf16[1,4096,512]{2,1,0:T(8,128)(2,1)}, u32[]{:S(2)}) copy-start(bf16[1,4096,512]{2,1,0:T(8,128)(2,1)} %param.26) | copy-start | bytes 12582916
  203.1 2.4 copy-start.1
  205.5 6.0 %copy-start.17 = (f32[1,128,4]{1,2,0:T(4,128)S(1)}, f32[1,128,4]{1,2,0:T(4,128)}, u32[]{:S(2)}) copy-start(f32[1,128,4]{1,2,0:T(4,128)} %param.24) | copy-start | bytes 6148
  205.5 70.2 %copy-start.11 = (s32[512]{0:T(512)S(1)}, s32[512]{0:T(512)}, u32[]{:S(2)}) copy-start(s32[512]{0:T(512)} %multiply_add_fusion.target_ref) | copy-start | bytes 6148
  205.5 70.2 %all-to-all-start.3 = ((bf16[128,160,128]{2,1,0:T(8,128)(2,1)}), bf16[128,160,128]{2,1,0:T(8,128)(2,1)}, u32[]{:S(2)}, u32[]{:S(2)}) async-start(bf16[128,160,128]{2,1,0:T(8,128)(2,1)} %bitcast.35), calls=%async_computation.3 | async-start | bytes 10485760 | tf_op jit(solution)/shard_map/all_to_all | solution.py:424

commit v3 on v2

--- a/solution.py
+++ b/solution.py
@@ -34,20 +34,17 @@
 
 def gate_terms(forget, free):
     leak = free * jax.nn.sigmoid(-forget.astype(F32))
-    causal = jnp.where(tril(leak.shape[0]), 1.0, 0.0)
-    log_run = dot(causal, jnp.log1p(-leak), precision=lax.Precision.HIGHEST)
+    causal = jnp.where(tril(leak.shape[0]), 1.0, 0.0).astype(BF16)
+    log_keep = jnp.log1p(-leak)
+    high = log_keep.astype(BF16)
+    rest = log_keep - high.astype(F32)
+    mid, low = split(rest)
+    log_run = (dot(causal, low) + dot(causal, mid)) + dot(causal, high)
     return leak, log_run
 
 
-def pair_kernel(forget_ref, value_ref, out_ref):
-    size = out_ref.shape[3]
-    for h in range(out_ref.shape[0]):
-        out_ref[h, 0] = forget_ref[:, h * size : (h + 1) * size]
-        out_ref[h, 1] = value_ref[:, h * size : (h + 1) * size]
-
-
-def state_kernel(pair_ref, bound_ref, before_ref):
-    blocks, _, rows, size = pair_ref.shape
+def pair_kernel(forget_ref, value_ref, bound_ref, out_ref):
+    rows, size = forget_ref.shape[0], out_ref.shape[2]
     free = 1.0 - bound_ref[...]
     high = free.astype(BF16).astype(F32)
     mid = (free - high).astype(BF16).astype(F32)
@@ -56,21 +53,30 @@
     tail = jnp.where(
         row == 0, high, jnp.where(row == 1, mid, jnp.where(row == 2, low, 0.0))
     ).astype(BF16)
+    for h in range(out_ref.shape[0]):
+        out_ref[h, 0:rows] = forget_ref[:, h * size : (h + 1) * size]
+        out_ref[h, rows : 2 * rows] = value_ref[:, h * size : (h + 1) * size]
+        out_ref[h, 2 * rows : 2 * rows + MSG_PAD] = tail
+
+
+def state_kernel(pair_ref, bound_ref, before_ref):
+    blocks, _, size = pair_ref.shape
+    rows = (pair_ref.shape[1] - MSG_PAD) // 2
+    free = 1.0 - bound_ref[...]
     group = 4
 
     def some(i, state):
-        forget = jnp.concatenate([pair_ref[i * group + j, 0] for j in range(group)], axis=1)
+        forget = jnp.concatenate([pair_ref[i * group + j, 0:rows] for j in range(group)], axis=1)
         leak, log_run = gate_terms(forget, jnp.concatenate([free] * group, axis=1))
         log_last = log_run[rows - 1 : rows, :]
         carry = leak * jnp.exp(log_last - log_run)
         keep = jnp.exp(log_last)
         for j in range(group):
             n = i * group + j
-            before_ref[n, 0:size, :] = state.astype(BF16)
-            before_ref[n, size : size + MSG_PAD, :] = tail
+            before_ref[n] = state.astype(BF16)
             at = slice(j * size, (j + 1) * size)
             upper, lower = split(carry[:, at])
-            value = pair_ref[n, 1]
+            value = pair_ref[n, rows : 2 * rows]
             push = dot(value, upper, ((0,), (0,))) + dot(value, lower, ((0,), (0,)))
             state = keep[:, at] * state + push
         return state
@@ -78,18 +84,18 @@
     lax.fori_loop(0, blocks // group, some, jnp.zeros((size, size), F32))
 
 
-def mix_kernel(query_ref, forget_ref, value_ref, gate_ref, before_ref, gain_ref, out_ref):
-    heads, _, size = before_ref.shape
-    tails = [before_ref[h, size : size + MSG_PAD, :].astype(F32) for h in range(heads)]
+def within_kernel(query_ref, forget_ref, value_ref, tail_ref, mix_ref, high_ref, low_ref):
+    heads, _, size = tail_ref.shape
+    tails = [tail_ref[h].astype(F32) for h in range(heads)]
     free = jnp.concatenate([t[2:3] + t[1:2] + t[0:1] for t in tails], axis=1)
     leak, log_run = gate_terms(forget_ref[...], free)
     q_scaled = query_ref[...].astype(F32) * jnp.exp(log_run)
     k_scaled = leak * jnp.exp(-log_run)
     q_high, q_low = split(q_scaled)
     k_high, k_low = split(k_scaled)
+    high_ref[...] = q_high
+    low_ref[...] = q_low
     causal = tril(leak.shape[0])
-    u = gate_ref[...].astype(F32)
-    silu = u / (1.0 + jnp.exp(-u))
     lanes = ((1,), (1,))
     for h in range(heads):
         at = slice(h * size, (h + 1) * size)
@@ -100,36 +106,48 @@
         )
         s_high, s_low = split(jnp.where(causal, scores, 0.0))
         value = value_ref[:, at]
-        before = before_ref[h, 0:size, :]
+        mix_ref[:, at] = dot(s_high, value) + dot(s_low, value)
+
+
+def finish_kernel(first, mix_ref, high_ref, low_ref, gate_ref, before_ref, gain_ref, out_ref):
+    size = before_ref.shape[2]
+    lanes = ((1,), (1,))
+    for h in range(out_ref.shape[1] // size):
+        to = slice(h * size, (h + 1) * size)
+        at = slice((first + h) * size, (first + h + 1) * size)
+        before = before_ref[first + h]
         mix = (
-            dot(s_high, value)
-            + dot(s_low, value)
-            + dot(q_high[:, at], before, lanes)
-            + dot(q_low[:, at], before, lanes)
+            mix_ref[:, at]
+            + dot(high_ref[:, at], before, lanes)
+            + dot(low_ref[:, at], before, lanes)
         )
         scale = lax.rsqrt(jnp.mean(mix * mix, axis=-1, keepdims=True) + NORM_EPS)
         normed = (mix * scale * gain_ref[...]).astype(BF16)
-        out_ref[:, at] = (normed.astype(F32) * silu[:, at]).astype(BF16)
-
-
-def block_products(rows_ref, refs):
-    at, total = 0, None
-    for w_ref in refs:
-        depth = w_ref.shape[0]
-        part = dot(rows_ref[:, at : at + depth], w_ref[...])
-        total = part if total is None else total + part
-        at += depth
-        if at == rows_ref.shape[1]:
-            yield total.astype(BF16)
-            at, total = 0, None
-
-
-def columns_kernel(mine_ref, other_ref, *refs):
-    *w_refs, keep_ref, give_ref = refs
+        u = gate_ref[:, at].astype(F32)
+        out_ref[:, to] = (normed.astype(F32) * (u / (1.0 + jnp.exp(-u)))).astype(BF16)
+
+
+def columns_kernel(place_ref, mine_a, mine_b, other_a, other_b, *refs):
+    *w_refs, keep_ref, give_ref, mine_ref, other_ref = refs
     columns = w_refs[0].shape[1]
+    depth = mine_ref.shape[1]
+    half = mine_a.shape[1]
+    mine_ref[:, :half], mine_ref[:, half:] = mine_a[...], mine_b[...]
+    other_ref[:, :half], other_ref[:, half:] = other_a[...], other_b[...]
     for src, dst in ((mine_ref, keep_ref), (other_ref, give_ref)):
-        for n, block in enumerate(block_products(src, w_refs)):
-            dst[:, n * columns : (n + 1) * columns] = block
+        n, done, total = 0, 0, None
+        for i, w_ref in enumerate(w_refs):
+            rows = w_ref.shape[0]
+            if rows == depth:
+                part = dot(src[...], w_ref[...])
+            else:
+                at = pl.multiple_of(place_ref[i] * rows, rows)
+                part = dot(src[:, pl.ds(at, rows)], w_ref[...])
+            total = part if total is None else total + part
+            done += rows
+            if done == depth:
+                dst[:, n * columns : (n + 1) * columns] = total.astype(BF16)
+                n, done, total = n + 1, 0, None
 
 
 def route_kernel(slot_ref, order_ref, *refs):
@@ -274,16 +292,22 @@
     experts = expert_gate.shape[0] * span
     slots = experts * CAPACITY
 
-    half = channels // 2
-    upper, lower = out_weight[:half], out_weight[half:]
     ring = lax.axis_size("dp")
-    forward = [(d, (d + 2) % ring) for d in range(ring)]
-    backward = [(d, (d + ring - 2) % ring) for d in range(ring)]
+    turn = 4
+    along = lax.axis_index("sp") % turn
     across = [(d, d ^ 1) for d in range(ring)]
-    before_upper = lax.ppermute(upper, "dp", forward)
-    after_lower = lax.ppermute(lower, "dp", backward)
-    before_lower = lax.ppermute(lower, "dp", forward)
-    after_upper = lax.ppermute(upper, "dp", backward)
+
+    def hop(x, chips):
+        return lax.ppermute(x, "dp", [(d, (d + 2 * chips) % ring) for d in range(ring)])
+
+    def pass_on(x, steps):
+        moves = [(s, s // turn * turn + (s + steps) % turn) for s in range(lax.axis_size("sp"))]
+        return lax.ppermute(x, "sp", moves)
+
+    quarter = channels // turn
+    far = hop(lax.dynamic_slice_in_dim(out_weight, along * quarter, quarter), 2)
+    before_block = hop(out_weight, 1)
+    after_block = hop(out_weight, -1)
 
     def swap(x):
         return lax.ppermute(x, "dp", across)
@@ -293,56 +317,67 @@
     f = forget_pre.reshape(tokens, channels)
     v = values.reshape(tokens, channels)
     g = out_gate.reshape(tokens, channels)
+    bound = lower_bound.reshape(1, size)
+    message = 2 * tokens + MSG_PAD
     pair = pl.pallas_call(
         pair_kernel,
-        in_specs=[in_vmem, in_vmem],
+        in_specs=[in_vmem] * 3,
         out_specs=in_vmem,
-        out_shape=jax.ShapeDtypeStruct((heads, 2, tokens, size), BF16),
+        out_shape=jax.ShapeDtypeStruct((heads, message, size), BF16),
         cost_estimate=cost(1e6, 2e6),
-        compiler_params=pltpu.CompilerParams(vmem_limit_bytes=8 * 2**20),
+        compiler_params=pltpu.CompilerParams(vmem_limit_bytes=60 * 2**20),
         name="pair",
-    )(f, v)
+    )(f, v, bound)
     arrived = lax.all_to_all(pair, "sp", split_axis=0, concat_axis=0, tiled=True)
-    arrived, before_upper, after_lower = lax.optimization_barrier(
-        (arrived, before_upper, after_lower)
-    )
-    far_upper = lax.ppermute(before_upper, "dp", forward)
-    far_lower = lax.ppermute(after_lower, "dp", backward)
+    far_parts = (far, pass_on(far, 1), pass_on(far, -1), pass_on(far, 2))
     before = pl.pallas_call(
         state_kernel,
         in_specs=[in_vmem, in_vmem],
         out_specs=in_vmem,
-        out_shape=jax.ShapeDtypeStruct((arrived.shape[0], size + MSG_PAD, size), BF16),
+        out_shape=jax.ShapeDtypeStruct((arrived.shape[0], size, size), BF16),
         cost_estimate=cost(1e9, 2e6),
         compiler_params=pltpu.CompilerParams(vmem_limit_bytes=12 * 2**20),
         name="state",
-    )(arrived, lower_bound.reshape(1, size))
+    )(arrived, bound)
     before = lax.all_to_all(before, "sp", split_axis=0, concat_axis=0, tiled=True)
-    before, before_lower, after_upper = lax.optimization_barrier(
-        (before, before_lower, after_upper)
-    )
     target, slot_owner = slots_of(
         routing.reshape(tokens * top_count), experts, CAPACITY, tokens, top_count
     )
     per_step = 4
     head_block = pl.BlockSpec((tokens, per_step * size), lambda h: (0, h))
-    gated = pl.pallas_call(
-        mix_kernel,
+    mix_shape = jax.ShapeDtypeStruct((tokens, channels), F32)
+    q_shape = jax.ShapeDtypeStruct((tokens, channels), BF16)
+    mix, q_high, q_low = pl.pallas_call(
+        within_kernel,
         grid=(heads // per_step,),
-        in_specs=[head_block] * 4
-        + [
-            pl.BlockSpec((per_step, size + MSG_PAD, size), lambda h: (h, 0, 0)),
-            pl.BlockSpec((1, size), lambda h: (0, 0)),
-        ],
-        out_specs=head_block,
-        out_shape=jax.ShapeDtypeStruct((tokens, channels), BF16),
+        in_specs=[head_block] * 3
+        + [pl.BlockSpec((per_step, MSG_PAD, size), lambda h: (h, 2 * tokens // MSG_PAD, 0))],
+        out_specs=[head_block] * 3,
+        out_shape=[mix_shape, q_shape, q_shape],
         cost_estimate=cost(2e9, 3e6),
-        compiler_params=pltpu.CompilerParams(vmem_limit_bytes=60 * 2**20),
-        name="mix",
-    )(q, f, v, g, before, head_gain.reshape(1, size))
-
-    gated, slot_owner, target = lax.optimization_barrier((gated, slot_owner, target))
-    gated_other = swap(gated)
+        compiler_params=pltpu.CompilerParams(vmem_limit_bytes=16 * 2**20),
+        name="within",
+    )(q, f, v, arrived)
+
+    def finish(first, count):
+        return pl.pallas_call(
+            functools.partial(finish_kernel, first),
+            in_specs=[in_vmem] * 6,
+            out_specs=in_vmem,
+            out_shape=jax.ShapeDtypeStruct((tokens, count * size), BF16),
+            cost_estimate=cost(6e8, 2e6),
+            compiler_params=pltpu.CompilerParams(vmem_limit_bytes=12 * 2**20),
+            name="finish",
+        )(mix, q_high, q_low, g, before, head_gain.reshape(1, size))
+
+    weights = route_weight.reshape(tokens * top_count)
+    gated_a = finish(0, heads // 2)
+    other_a = swap(gated_a)
+    gated_b = finish(heads // 2, heads // 2)
+    gated_b, slot_owner, target, weights = lax.optimization_barrier(
+        (gated_b, slot_owner, target, weights)
+    )
+    other_b = swap(gated_b)
     columns = out_weight.shape[1]
 
     def project(limit, *parts):
@@ -350,17 +385,19 @@
         shape = jax.ShapeDtypeStruct((tokens, wide), BF16)
         keep, give = pl.pallas_call(
             columns_kernel,
-            in_specs=[in_vmem] * (2 + len(parts)),
+            in_specs=[whole(None, pltpu.SMEM)] + [in_vmem] * (4 + len(parts)),
             out_specs=[in_vmem] * 2,
             out_shape=[shape] * 2,
+            scratch_shapes=[pltpu.VMEM((tokens, channels), BF16)] * 2,
             cost_estimate=cost(4 * tokens * channels * wide, 2 * channels * wide),
             compiler_params=pltpu.CompilerParams(vmem_limit_bytes=limit * 2**20),
-        )(gated, gated_other, *parts)
+        )(place, gated_a, gated_b, other_a, other_b, *parts)
         return keep, swap(give)
 
-    near = project(14, out_weight, before_upper, before_lower, after_upper, after_lower)
-    near, far_upper, far_lower = lax.optimization_barrier((near, far_upper, far_lower))
-    far = project(8, far_upper, far_lower)
+    place = jnp.stack([(along + turn - shift) % turn for shift in (0, 1, turn - 1, 2)])
+    place = place.astype(jnp.int32)
+    near = project(14, out_weight, before_block, after_block)
+    far = project(8, *far_parts)
     chip, core = lax.axis_index("dp") // 2, lax.axis_index("dp") % 2
     order = jnp.stack(
         [
@@ -436,7 +473,7 @@
         cost_estimate=cost(4e8, 8e6),
         compiler_params=pltpu.CompilerParams(vmem_limit_bytes=16 * 2**20),
         name="combine",
-    )(target, route_weight.reshape(tokens * top_count), back, hidden)
+    )(target, weights, back, hidden)
     return out.reshape(1, tokens, width)
 
 

time: 281 us -> 254 us (0.904)
  waiting for transfers between devices: 122 us -> 30.7 us
  blocking collectives: 68.8 us -> 141 us
  starting transfers between devices: 34.6 us -> 27.5 us
  Pallas kernels: 36.5 us -> 39.4 us
    all_to_all x0 -> x1, blocking collectives: none -> 68.2 us  [local(): back = exchange(results.reshape(chunk)).reshape(slots, pieces, LANES)]
    all_to_all x1 -> x0, waiting for transfers between devices: 63.9 us -> none  [local(): back = exchange(results.reshape(chunk)).reshape(slots, pieces, LANES)]
    ppermute x6, waiting for transfers between devices: 38.1 us -> 15.4 us  [the longest x3 13.4 us: pass_on(): return lax.ppermute(x, 'sp', moves)]
    all_to_all x1, waiting for transfers between devices: 6.94 us -> 0.01 us  [local(): lax.all_to_all(before, 'sp', split_axis=0, concat_axis=0, tiled=True)]
    all_to_all x1 -> x0, starting transfers between devices: 5.99 us -> none  [local(): back = exchange(results.reshape(chunk)).reshape(slots, pieces, LANES)]
    pallas_call x4 -> x6, Pallas kernels: 12.7 us -> 16.5 us  [the longest x2 6.82 us: project(): pl.pallas_call(columns_kernel, in_specs=[whole(None, pltpu.SMEM)] + [in_v...]
    all_to_all x1, blocking collectives: 68.8 us -> 72.6 us  [local(): rows_in = exchange(outgoing.reshape(chunk)).reshape(slots, pieces, LANES)]
    slice x1 -> x0, local copies, waits for them, and re-layouts: 3.06 us -> none  [local(): upper, lower = (out_weight[:half], out_weight[half:])]
  transfers between devices with their start and end apart: 12 -> 12, of which waited for: 6 -> 5; matrix products, arithmetic and copies ran while one was open for 2% -> 2% of each run, Pallas kernels for 3% -> 8%
where the time goes in v3:
time: 254 us
  blocking collectives  141 us (56%)
  Pallas kernels  39.4 us (16%)
  waiting for transfers between devices  30.7 us (12%)
  starting transfers between devices  27.5 us (11%)
  local copies, waits for them, and re-layouts  14.2 us (6%)
    all_to_all x1, blocking collectives, local(): rows_in = exchange(outgoing.reshape(chunk)).reshape(slots, pieces, LANES)  72.6 us
    all_to_all x1, blocking collectives, local(): back = exchange(results.reshape(chunk)).reshape(slots, pieces, LANES)  68.2 us
    all_to_all x1, waiting for transfers between devices, local(): lax.all_to_all(pair, 'sp', split_axis=0, concat_axis=0, tiled=True)  14.4 us
    ppermute x3, waiting for transfers between devices, pass_on(): return lax.ppermute(x, 'sp', moves)  13.4 us
    pallas_call x1, Pallas kernels, local(): pl.pallas_call(expert_kernel, in_specs=[in_vmem] * 4, out_specs=in_vmem,...  13 us
    unnamed x42, local copies, waits for them, and re-layouts  9.05 us
    all_to_all x1, starting transfers between devices, local(): lax.all_to_all(pair, 'sp', split_axis=0, concat_axis=0, tiled=True)  7.6 us
    pallas_call x2, Pallas kernels, project(): pl.pallas_call(columns_kernel, in_specs=[whole(None, pltpu.SMEM)] + [in_v...  6.82 us
  transfers between devices with their start and end apart: 12, of which 5 were waited for; matrix products, arithmetic and copies ran while one was open for 2% of the time, Pallas kernels for 8%

profile of v3, /device:TPU:1, one launch (start us, length us, event | category | flops | bytes accessed | tf_op | source)
XLA Modules:
  0.0 253.5 jit_solution(3293283307711609319)
XLA Ops:
  0.0 3.6 %collective-permute-start.3 = (bf16[2048,512]{1,0:T(8,128)(2,1)}, bf16[2048,512]{1,0:T(8,128)(2,1)}, u32[]{:S(2)}, u32[]{:S(2)}) collective-permute-start(bf16[2048,512]{1,0:T(8,128)(2,1)} %refs_0_.1), channel_id=1, source_target_pairs={{0,6},{1,7},{2,0},{3,1},{4,2},{5,3},{6,4},{7,5},{8,14},{9,15},{10,... | collective-permute-start | bytes 6291464 | tf_op jit(solution)/shard_map/ppermute | solution.py:301
  3.6 1.9 constant_dynamic-slice_fusion
  5.6 1.6 collective-permute-start.5
  7.2 2.4 pair.1
  9.6 7.6 %all-to-all-start = ((bf16[16,272,128]{2,1,0:T(8,128)(2,1)}), bf16[16,272,128]{2,1,0:T(8,128)(2,1)S(1)}, u32[]{:S(2)}, u32[]{:S(2)}) async-start(bf16[16,272,128]{2,1,0:T(8,128)(2,1)} %pair.1), calls=%async_computation | async-start | bytes 2228224 | tf_op jit(solution)/shard_map/all_to_all | solution.py:331
  17.2 0.1 copy.16
  17.4 0.1 eq.40
  17.5 0.1 eq.44
  17.6 0.1 copy.15
  17.7 0.1 mul.44
  17.8 0.1 copy.18
  17.9 0.1 copy.20
  18.0 0.1 reshape.107.weight_ref
  18.1 0.2 fusion.1
  18.5 0.2 fusion
  18.7 14.4 %all-to-all-done.tail_ref.pair_ref = bf16[16,272,128]{2,1,0:T(8,128)(2,1)S(1)} async-done(((bf16[16,272,128]{2,1,0:T(8,128)(2,1)}), bf16[16,272,128]{2,1,0:T(8,128)(2,1)S(1)}, u32[]{:S(2)}, u32[]{:S(2)}) %all-to-all-start) | async-done | bytes 1114144 | tf_op jit(solution)/shard_map/all_to_all | solution.py:331
  33.1 3.4 %state.1 = bf16[16,128,128]{2,1,0:T(8,128)(2,1)} custom-call(bf16[16,272,128]{2,1,0:T(8,128)(2,1)S(1)} %all-to-all-done.tail_ref.pair_ref, f32[1,128]{1,0:T(1,128)S(1)} %bitcast.53), custom_call_target="tpu_custom_call" | custom-call | flops 1000000000 | bytes 2000000 | tf_op jit(solution)/shard_map/state/pallas_call | solution.py:333
  36.5 5.0 %all-to-all-start.1 = ((bf16[16,128,128]{2,1,0:T(8,128)(2,1)}), bf16[16,128,128]{2,1,0:T(8,128)(2,1)S(1)}, u32[]{:S(2)}, u32[]{:S(2)}) async-start(bf16[16,128,128]{2,1,0:T(8,128)(2,1)} %state.1), calls=%async_computation.1 | async-start | bytes 1048576 | tf_op jit(solution)/shard_map/all_to_all | solution.py:342
  41.6 2.4 scatter_custom_fusion.slot_ref
  44.0 1.2 copy-done.5
  45.3 1.0 copy-done.7
  46.3 1.0 copy-done.8
  47.4 1.0 copy-done.17
  48.4 6.0 %within.1 = (f32[128,2048]{1,0:T(8,128)S(1)}, bf16[128,2048]{1,0:T(8,128)(2,1)S(1)}, bf16[128,2048]{1,0:T(8,128)(2,1)S(1)}) custom-call(bf16[128,2048]{1,0:T(8,128)(2,1)S(1)} %bitcast.57, bf16[128,2048]{1,0:T(8,128)(2,1)S(1)} %bitcast.46, bf16[128,2048]{1,0:T(8,128)(2,1)S(1)} %bitcast.48, bf16[16,272,128]{2,1,0:T(8,128)(2,1)S(1)} %copy-done.5), custom_call_target="tpu_custom_call" | custom-call | flops 2000000000 | bytes 3000000 | tf_op jit(solution)/shard_map/within/pallas_call | solution.py:350
  54.5 0.8 copy-done.2
  55.3 1.0 copy-done.3
  56.3 0.6 finish.2.mine_b
  56.9 2.0 collective-permute-start.1
  58.9 0.6 finish.3.mine_a
  59.6 0.1 collective-permute-start
  59.7 2.0 collective-permute-done.5.refs_0_
  61.6 2.7 %collective-permute-start.8 = (bf16[512,512]{1,0:T(8,128)(2,1)}, bf16[512,512]{1,0:T(8,128)(2,1)S(1)}, u32[]{:S(2)}, u32[]{:S(2)}) collective-permute-start(bf16[512,512]{1,0:T(8,128)(2,1)} %collective-permute-done.5.refs_0_), channel_id=1, source_target_pairs={{0,16},{8,24},{16,0},{24,8},{32,48},{40,56},{48,32},{56,40},{64,80... | collective-permute-start | bytes 1572872 | tf_op jit(solution)/shard_map/ppermute | solution.py:305
  64.4 0.9 collective-permute-start.7
  65.3 0.6 collective-permute-start.6
  66.0 1.6 copy-done
  67.5 4.9 %shard_map.136 = (bf16[128,1536]{1,0:T(8,128)(2,1)S(1)}, bf16[128,1536]{1,0:T(8,128)(2,1)}) custom-call(s32[4]{0:T(128)S(1)} %pad_add_fusion.place_ref, bf16[128,1024]{1,0:T(8,128)(2,1)S(1)} %finish.3.mine_a, bf16[128,1024]{1,0:T(8,128)(2,1)S(1)} %finish.2.mine_b, bf16[128,1024]{1,0:T(8,128)(2,1)S(1)} %collective-permute-done.other_a, ...), custom_call_target="tpu_custom_call" | custom-call | flops 1610612736 | bytes 6291456 | tf_op jit(solution)/shard_map/pallas_call | solution.py:386
  72.4 2.7 %collective-permute-start.4 = (bf16[128,1536]{1,0:T(8,128)(2,1)}, bf16[128,1536]{1,0:T(8,128)(2,1)}, u32[]{:S(2)}, u32[]{:S(2)}) collective-permute-start(bf16[128,1536]{1,0:T(8,128)(2,1)} %get-tuple-element.26), channel_id=1, source_target_pairs={{0,1},{1,0},{2,3},{3,2},{4,5},{5,4},{6,7},{7,6},{8,9},{9,8},{10,11... | collective-permute-start | bytes 1179656 | tf_op jit(solution)/shard_map/ppermute | solution.py:313
  75.1 12.5 %collective-permute-done.7.refs_2_ = bf16[512,512]{1,0:T(8,128)(2,1)S(1)} collective-permute-done((bf16[512,512]{1,0:T(8,128)(2,1)}, bf16[512,512]{1,0:T(8,128)(2,1)S(1)}, u32[]{:S(2)}, u32[]{:S(2)}) %collective-permute-start.7) | collective-permute-done | bytes 524320 | tf_op jit(solution)/shard_map/ppermute | solution.py:305
  87.6 0.9 collective-permute-done.6.refs_1_
  88.5 1.9 shard_map.137
  90.5 0.6 collective-permute-start.9
  91.2 0.9 collective-permute-done.9.refs_3_
  92.1 1.0 copy-done.10
  93.1 3.5 %route.1 = (bf16[640,32,128]{2,1,0:T(8,128)(2,1)S(1)}, bf16[128,32,128]{2,1,0:T(8,128)(2,1)S(1)}) custom-call(s32[640]{0:T(1024)S(1)} %scatter_custom_fusion.slot_ref, s32[8]{0:T(128)S(1)} %stack.50.order_ref, bf16[128,1536]{1,0:T(8,128)(2,1)S(1)} %copy-done.10, bf16[128,1536]{1,0:T(8,128)(2,1)} %collective-permute-done.4.refs_1_, ...), custom_call_target="tpu_custom_call" | custom-call | flops 40000000 | bytes 12000000 | tf_op jit(solution)/shard_map/route/pallas_call | solution.py:411
  96.6 72.6 %all_to_all.20 = bf16[128,160,128]{2,1,0:T(8,128)(2,1)} all-to-all(bf16[128,160,128]{2,1,0:T(8,128)(2,1)S(1)} %bitcast.40), channel_id=1, replica_groups=mesh['sp'=16,'dp'=8] {'sp','dp'}, dimensions={0} | all-to-all | bytes 10485760 | tf_op jit(solution)/shard_map/all_to_all | solution.py:440
  169.3 13.0 %expert.1 = bf16[640,32,128]{2,1,0:T(8,128)(2,1)S(1)} custom-call(bf16[640,32,128]{2,1,0:T(8,128)(2,1)} %bitcast.58, bf16[4096,512]{1,0:T(8,128)(2,1)S(1)} %bitcast.54, bf16[4096,512]{1,0:T(8,128)(2,1)S(1)} %bitcast.55, bf16[512,4096]{1,0:T(8,128)(2,1)S(1)} %bitcast.56), custom_call_target="tpu_custom_call" | custom-call | flops 8000000000 | bytes 24000000 | tf_op jit(solution)/shard_map/expert/pallas_call | solution.py:443
  182.3 68.2 %all_to_all.21 = bf16[128,160,128]{2,1,0:T(8,128)(2,1)S(1)} all-to-all(bf16[128,160,128]{2,1,0:T(8,128)(2,1)S(1)} %bitcast.41), channel_id=1, replica_groups=mesh['sp'=16,'dp'=8] {'sp','dp'}, dimensions={0} | all-to-all | bytes 10485760 | tf_op jit(solution)/shard_map/all_to_all | solution.py:461
  250.5 3.0 %combine.1 = bf16[128,4096]{1,0:T(8,128)(2,1)} custom-call(s32[512]{0:T(512)S(1)} %multiply_add_fusion.target_ref, f32[512]{0:T(512)S(1)} %reshape.107.weight_ref, bf16[640,32,128]{2,1,0:T(8,128)(2,1)S(1)} %bitcast.39, bf16[128,32,128]{2,1,0:T(8,128)(2,1)S(1)} %get-tuple-element.30.hidden_ref), custom_call_target="tpu_custom_call" | custom-call | flops 400000000 | bytes 8000000 | tf_op jit(solution)/shard_map/combine/pallas_call | solution.py:462
  (51 shorter events, 0.4 us)
Async XLA Ops:
  0.0 33.1 %copy-start.13 = (f32[128]{0:T(128)S(1)}, f32[128]{0:T(128)}, u32[]{:S(2)}) copy-start(f32[128]{0:T(128)} %param.18) | copy-start | bytes 1540
  0.0 17.2 %copy-start.18 = (s32[1,128,4]{1,2,0:T(4,128)S(1)}, s32[1,128,4]{1,2,0:T(4,128)}, u32[]{:S(2)}) copy-start(s32[1,128,4]{1,2,0:T(4,128)} %param.23) | copy-start | bytes 6148
  0.0 17.9 %copy-start.19 = (f32[1,128,4]{1,2,0:T(4,128)S(1)}, f32[1,128,4]{1,2,0:T(4,128)}, u32[]{:S(2)}) copy-start(f32[1,128,4]{1,2,0:T(4,128)} %param.24) | copy-start | bytes 6148
  0.0 65.9 %collective-permute-start.3 = (bf16[2048,512]{1,0:T(8,128)(2,1)}, bf16[2048,512]{1,0:T(8,128)(2,1)}, u32[]{:S(2)}, u32[]{:S(2)}) collective-permute-start(bf16[2048,512]{1,0:T(8,128)(2,1)} %refs_0_.1), channel_id=1, source_target_pairs={{0,6},{1,7},{2,0},{3,1},{4,2},{5,3},{6,4},{7,5},{8,14},{9,15},{10,... | collective-permute-start | bytes 6291464 | tf_op jit(solution)/shard_map/ppermute | solution.py:301
  3.6 62.3 %collective-permute-start.2 = (bf16[2048,512]{1,0:T(8,128)(2,1)}, bf16[2048,512]{1,0:T(8,128)(2,1)}, u32[]{:S(2)}, u32[]{:S(2)}) collective-permute-start(bf16[2048,512]{1,0:T(8,128)(2,1)} %refs_0_.1), channel_id=1, source_target_pairs={{0,2},{1,3},{2,4},{3,5},{4,6},{5,7},{6,0},{7,1},{8,10},{9,11},{10,... | collective-permute-start | bytes 6291464 | tf_op jit(solution)/shard_map/ppermute | solution.py:301
  5.6 56.1 %collective-permute-start.5 = (bf16[512,512]{1,0:T(8,128)(2,1)}, bf16[512,512]{1,0:T(8,128)(2,1)}, u32[]{:S(2)}, u32[]{:S(2)}) collective-permute-start(bf16[512,512]{1,0:T(8,128)(2,1)} %constant_dynamic-slice_fusion), channel_id=1, source_target_pairs={{0,4},{1,5},{2,6},{3,7},{4,0},{5,1},{6,2},{7,3},{8,12},{9,13},{10,... | collective-permute-start | bytes 1572872 | tf_op jit(solution)/shard_map/ppermute | solution.py:301
  9.6 23.5 %all-to-all-start = ((bf16[16,272,128]{2,1,0:T(8,128)(2,1)}), bf16[16,272,128]{2,1,0:T(8,128)(2,1)S(1)}, u32[]{:S(2)}, u32[]{:S(2)}) async-start(bf16[16,272,128]{2,1,0:T(8,128)(2,1)} %pair.1), calls=%async_computation | async-start | bytes 2228224 | tf_op jit(solution)/shard_map/all_to_all | solution.py:331
  33.1 3.4 %copy-start.4 = (bf16[16,272,128]{2,1,0:T(8,128)(2,1)}, bf16[16,272,128]{2,1,0:T(8,128)(2,1)S(1)}, u32[]{:S(2)}) copy-start(bf16[16,272,128]{2,1,0:T(8,128)(2,1)S(1)} %all-to-all-done.tail_ref.pair_ref) | copy-start | bytes 3342340
  36.5 18.7 %copy-start.1 = (bf16[1,128,2048]{2,1,0:T(8,128)(2,1)S(1)}, bf16[1,128,2048]{2,1,0:T(8,128)(2,1)}, u32[]{:S(2)}) copy-start(bf16[1,128,2048]{2,1,0:T(8,128)(2,1)} %param.17) | copy-start | bytes 1572868
  36.5 18.7 %copy-start.12 = (f32[128]{0:T(128)S(1)}, f32[128]{0:T(128)}, u32[]{:S(2)}) copy-start(f32[128]{0:T(128)} %param.19) | copy-start | bytes 1540
  36.5 18.7 %all-to-all-start.1 = ((bf16[16,128,128]{2,1,0:T(8,128)(2,1)}), bf16[16,128,128]{2,1,0:T(8,128)(2,1)S(1)}, u32[]{:S(2)}, u32[]{:S(2)}) async-start(bf16[16,128,128]{2,1,0:T(8,128)(2,1)} %state.1), calls=%async_computation.1 | async-start | bytes 1048576 | tf_op jit(solution)/shard_map/all_to_all | solution.py:342
  44.0 1.2 copy-start.5
  45.3 1.0 copy-start.7
  46.3 1.0 copy-start.8
  47.4 1.0 copy-start.17
  54.4 0.8 copy-start.2
  55.2 1.0 copy-start.3
  56.9 7.5 %collective-permute-start.1 = (bf16[128,1024]{1,0:T(8,128)(2,1)S(1)}, bf16[128,1024]{1,0:T(8,128)(2,1)S(1)}, u32[]{:S(2)}, u32[]{:S(2)}) collective-permute-start(bf16[128,1024]{1,0:T(8,128)(2,1)S(1)} %finish.2.mine_b), channel_id=1, source_target_pairs={{0,1},{1,0},{2,3},{3,2},{4,5},{5,4},{6,7},{7,6},{8,9},{9,8},{10,11... | collective-permute-start | bytes 786440 | tf_op jit(solution)/shard_map/ppermute | solution.py:313
  59.6 5.7 %collective-permute-start = (bf16[128,1024]{1,0:T(8,128)(2,1)S(1)}, bf16[128,1024]{1,0:T(8,128)(2,1)S(1)}, u32[]{:S(2)}, u32[]{:S(2)}) collective-permute-start(bf16[128,1024]{1,0:T(8,128)(2,1)S(1)} %finish.3.mine_a), channel_id=1, source_target_pairs={{0,1},{1,0},{2,3},{3,2},{4,5},{5,4},{6,7},{7,6},{8,9},{9,8},{10,11... | collective-permute-start | bytes 786440 | tf_op jit(solution)/shard_map/ppermute | solution.py:313
  61.6 13.5 %collective-permute-start.8 = (bf16[512,512]{1,0:T(8,128)(2,1)}, bf16[512,512]{1,0:T(8,128)(2,1)S(1)}, u32[]{:S(2)}, u32[]{:S(2)}) collective-permute-start(bf16[512,512]{1,0:T(8,128)(2,1)} %collective-permute-done.5.refs_0_), channel_id=1, source_target_pairs={{0,16},{8,24},{16,0},{24,8},{32,48},{40,56},{48,32},{56,40},{64,80... | collective-permute-start | bytes 1572872 | tf_op jit(solution)/shard_map/ppermute | solution.py:305
  64.4 23.2 %collective-permute-start.7 = (bf16[512,512]{1,0:T(8,128)(2,1)}, bf16[512,512]{1,0:T(8,128)(2,1)S(1)}, u32[]{:S(2)}, u32[]{:S(2)}) collective-permute-start(bf16[512,512]{1,0:T(8,128)(2,1)} %collective-permute-done.5.refs_0_), channel_id=1, source_target_pairs={{0,24},{8,0},{16,8},{24,16},{32,56},{40,32},{48,40},{56,48},{64,88... | collective-permute-start | bytes 1572872 | tf_op jit(solution)/shard_map/ppermute | solution.py:305
  65.3 23.3 %collective-permute-start.6 = (bf16[512,512]{1,0:T(8,128)(2,1)}, bf16[512,512]{1,0:T(8,128)(2,1)}, u32[]{:S(2)}, u32[]{:S(2)}) collective-permute-start(bf16[512,512]{1,0:T(8,128)(2,1)} %collective-permute-done.5.refs_0_), channel_id=1, source_target_pairs={{0,8},{8,16},{16,24},{24,0},{32,40},{40,48},{48,56},{56,32},{64,72... | collective-permute-start | bytes 1572872 | tf_op jit(solution)/shard_map/ppermute | solution.py:305
  65.9 1.6 copy-start
  67.5 24.6 %copy-start.6 = (bf16[1,128,4096]{2,1,0:T(8,128)(2,1)S(1)}, bf16[1,128,4096]{2,1,0:T(8,128)(2,1)}, u32[]{:S(2)}) copy-start(bf16[1,128,4096]{2,1,0:T(8,128)(2,1)} %param.20) | copy-start | bytes 3145732
  67.5 24.6 %copy-start.11 = (f32[4096]{0:T(1024)S(1)}, f32[4096]{0:T(1024)}, u32[]{:S(2)}) copy-start(f32[4096]{0:T(1024)} %param.22) | copy-start | bytes 49156
  72.4 18.1 %copy-start.9 = (bf16[128,1536]{1,0:T(8,128)(2,1)}, bf16[128,1536]{1,0:T(8,128)(2,1)S(1)}, u32[]{:S(2)}) copy-start(bf16[128,1536]{1,0:T(8,128)(2,1)S(1)} %get-tuple-element.25.refs_0_) | copy-start | bytes 1179652
  72.4 19.7 %collective-permute-start.4 = (bf16[128,1536]{1,0:T(8,128)(2,1)}, bf16[128,1536]{1,0:T(8,128)(2,1)}, u32[]{:S(2)}, u32[]{:S(2)}) collective-permute-start(bf16[128,1536]{1,0:T(8,128)(2,1)} %get-tuple-element.26), channel_id=1, source_target_pairs={{0,1},{1,0},{2,3},{3,2},{4,5},{5,4},{6,7},{7,6},{8,9},{9,8},{10,11... | collective-permute-start | bytes 1179656 | tf_op jit(solution)/shard_map/ppermute | solution.py:313
  90.5 1.6 collective-permute-start.9
  92.1 1.0 copy-start.10
  93.1 76.2 %copy-start.16 = (bf16[1,512,4096]{2,1,0:T(8,128)(2,1)S(1)}, bf16[1,512,4096]{2,1,0:T(8,128)(2,1)}, u32[]{:S(2)}) copy-start(bf16[1,512,4096]{2,1,0:T(8,128)(2,1)} %param.27) | copy-start | bytes 12582916
  96.6 72.7 %copy-start.14 = (bf16[1,4096,512]{2,1,0:T(8,128)(2,1)S(1)}, bf16[1,4096,512]{2,1,0:T(8,128)(2,1)}, u32[]{:S(2)}) copy-start(bf16[1,4096,512]{2,1,0:T(8,128)(2,1)} %param.25) | copy-start | bytes 12582916
  96.6 72.7 %copy-start.15 = (bf16[1,4096,512]{2,1,0:T(8,128)(2,1)S(1)}, bf16[1,4096,512]{2,1,0:T(8,128)(2,1)}, u32[]{:S(2)}) copy-start(bf16[1,4096,512]{2,1,0:T(8,128)(2,1)} %param.26) | copy-start | bytes 12582916

commit v4 on v3

--- a/solution.py
+++ b/solution.py
@@ -128,26 +128,36 @@
 
 
 def columns_kernel(place_ref, mine_a, mine_b, other_a, other_b, *refs):
-    *w_refs, keep_ref, give_ref, mine_ref, other_ref = refs
+    count = (len(refs) - 5) // 2
+    w_refs, buffers = refs[:count], refs[count + 4 : 2 * count + 4]
+    keep_ref, give_ref, mine_ref, other_ref = refs[count : count + 4]
+    sems = refs[-1]
+    copies = [
+        pltpu.make_async_copy(w, buffer, sems.at[i])
+        for i, (w, buffer) in enumerate(zip(w_refs, buffers))
+    ]
+    for copy in copies:
+        copy.start()
     columns = w_refs[0].shape[1]
     depth = mine_ref.shape[1]
     half = mine_a.shape[1]
     mine_ref[:, :half], mine_ref[:, half:] = mine_a[...], mine_b[...]
     other_ref[:, :half], other_ref[:, half:] = other_a[...], other_b[...]
-    for src, dst in ((mine_ref, keep_ref), (other_ref, give_ref)):
-        n, done, total = 0, 0, None
-        for i, w_ref in enumerate(w_refs):
-            rows = w_ref.shape[0]
+    n, done, totals = 0, 0, [0.0, 0.0]
+    for i, (copy, buffer) in enumerate(zip(copies, buffers)):
+        copy.wait()
+        rows = buffer.shape[0]
+        for k, src in enumerate((mine_ref, other_ref)):
             if rows == depth:
-                part = dot(src[...], w_ref[...])
+                totals[k] = dot(src[...], buffer[...])
             else:
                 at = pl.multiple_of(place_ref[i] * rows, rows)
-                part = dot(src[:, pl.ds(at, rows)], w_ref[...])
-            total = part if total is None else total + part
-            done += rows
-            if done == depth:
+                totals[k] = totals[k] + dot(src[:, pl.ds(at, rows)], buffer[...])
+        done += rows
+        if done == depth:
+            for total, dst in zip(totals, (keep_ref, give_ref)):
                 dst[:, n * columns : (n + 1) * columns] = total.astype(BF16)
-                n, done, total = n + 1, 0, None
+            n, done, totals = n + 1, 0, [0.0, 0.0]
 
 
 def route_kernel(slot_ref, order_ref, *refs):
@@ -294,7 +304,8 @@
 
     ring = lax.axis_size("dp")
     turn = 4
-    along = lax.axis_index("sp") % turn
+    at_z, at_x = lax.axis_index("sp") // turn, lax.axis_index("sp") % turn
+    along = (at_x + 2 * at_z) % turn
     across = [(d, d ^ 1) for d in range(ring)]
 
     def hop(x, chips):
@@ -303,6 +314,10 @@
     def pass_on(x, steps):
         moves = [(s, s // turn * turn + (s + steps) % turn) for s in range(lax.axis_size("sp"))]
         return lax.ppermute(x, "sp", moves)
+
+    def pass_up(x):
+        rows = lax.axis_size("sp")
+        return lax.ppermute(x, "sp", [(s, (s + turn) % rows) for s in range(rows)])
 
     quarter = channels // turn
     far = hop(lax.dynamic_slice_in_dim(out_weight, along * quarter, quarter), 2)
@@ -329,7 +344,7 @@
         name="pair",
     )(f, v, bound)
     arrived = lax.all_to_all(pair, "sp", split_axis=0, concat_axis=0, tiled=True)
-    far_parts = (far, pass_on(far, 1), pass_on(far, -1), pass_on(far, 2))
+    far_parts = (far, pass_on(far, 1), pass_on(far, -1), pass_up(far))
     before = pl.pallas_call(
         state_kernel,
         in_specs=[in_vmem, in_vmem],
@@ -355,7 +370,7 @@
         out_specs=[head_block] * 3,
         out_shape=[mix_shape, q_shape, q_shape],
         cost_estimate=cost(2e9, 3e6),
-        compiler_params=pltpu.CompilerParams(vmem_limit_bytes=16 * 2**20),
+        compiler_params=pltpu.CompilerParams(vmem_limit_bytes=60 * 2**20),
         name="within",
     )(q, f, v, arrived)
 
@@ -385,10 +400,14 @@
         shape = jax.ShapeDtypeStruct((tokens, wide), BF16)
         keep, give = pl.pallas_call(
             columns_kernel,
-            in_specs=[whole(None, pltpu.SMEM)] + [in_vmem] * (4 + len(parts)),
+            in_specs=[whole(None, pltpu.SMEM)]
+            + [in_vmem] * 4
+            + [whole(None, pl.ANY)] * len(parts),
             out_specs=[in_vmem] * 2,
             out_shape=[shape] * 2,
-            scratch_shapes=[pltpu.VMEM((tokens, channels), BF16)] * 2,
+            scratch_shapes=[pltpu.VMEM((tokens, channels), BF16)] * 2
+            + [pltpu.VMEM(p.shape, BF16) for p in parts]
+            + [pltpu.SemaphoreType.DMA((len(parts),))],
             cost_estimate=cost(4 * tokens * channels * wide, 2 * channels * wide),
             compiler_params=pltpu.CompilerParams(vmem_limit_bytes=limit * 2**20),
         )(place, gated_a, gated_b, other_a, other_b, *parts)
@@ -396,13 +415,13 @@
 
     place = jnp.stack([(along + turn - shift) % turn for shift in (0, 1, turn - 1, 2)])
     place = place.astype(jnp.int32)
-    near = project(14, out_weight, before_block, after_block)
-    far = project(8, *far_parts)
+    early = project(10, *far_parts, out_weight)
+    late = project(10, before_block, after_block)
     chip, core = lax.axis_index("dp") // 2, lax.axis_index("dp") % 2
     order = jnp.stack(
         [
             (chip + hop) % (ring // 2) * 2 + parity
-            for hops in ((0, ring // 2 - 1, 1), (2,))
+            for hops in ((2, 0), (ring // 2 - 1, 1))
             for parity in (core, 1 - core)
             for hop in hops
         ]
@@ -427,8 +446,8 @@
     )(
         slot_owner,
         order,
-        *near,
-        *far,
+        *early,
+        *late,
         residual.reshape(tokens, width),
         ffn_gain.reshape(1, width),
     )
@@ -450,7 +469,7 @@
             pltpu.VMEM((rows, width), BF16),
         ],
         cost_estimate=cost(8e9, 24e6),
-        compiler_params=pltpu.CompilerParams(vmem_limit_bytes=34 * 2**20),
+        compiler_params=pltpu.CompilerParams(vmem_limit_bytes=20 * 2**20),
         name="expert",
     )(
         rows_in,

time: 254 us -> 251 us (0.988)
  waiting for transfers between devices: 30.7 us -> 35.4 us
  local copies, waits for them, and re-layouts: 14.2 us -> 10.2 us
    ppermute x3, waiting for transfers between devices: 1.98 us -> 18.4 us  [hop(): lax.ppermute(x, 'dp', [(d, (d + 2 * chips) % ring) for d in range(ring)])]
    ppermute x3 -> x2, waiting for transfers between devices: 13.4 us -> 0.01 us  [pass_on(): return lax.ppermute(x, 'sp', moves)]
    unnamed x42 -> x34, local copies, waits for them, and re-layouts: 9.05 us -> 5.84 us
  transfers between devices with their start and end apart: 12 -> 12, of which waited for: 5 -> 5; matrix products, arithmetic and copies ran while one was open for 2% -> 2% of each run, Pallas kernels for 8% -> 9%
where the time goes in v4:
time: 251 us
  blocking collectives  140 us (56%)
  Pallas kernels  38.8 us (15%)
  waiting for transfers between devices  35.4 us (14%)
  starting transfers between devices  25.3 us (10%)
  local copies, waits for them, and re-layouts  10.2 us (4%)
    all_to_all x1, blocking collectives, local(): rows_in = exchange(outgoing.reshape(chunk)).reshape(slots, pieces, LANES)  71.8 us
    all_to_all x1, blocking collectives, local(): back = exchange(results.reshape(chunk)).reshape(slots, pieces, LANES)  68.2 us
    ppermute x3, waiting for transfers between devices, hop(): lax.ppermute(x, 'dp', [(d, (d + 2 * chips) % ring) for d in range(ring)])  18.4 us
    all_to_all x1, waiting for transfers between devices, local(): lax.all_to_all(pair, 'sp', split_axis=0, concat_axis=0, tiled=True)  14.4 us
    pallas_call x1, Pallas kernels, local(): pl.pallas_call(expert_kernel, in_specs=[in_vmem] * 4, out_specs=in_vmem,...  10.5 us
    pallas_call x1, Pallas kernels, local(): pl.pallas_call(within_kernel, grid=(heads // per_step,), in_specs=[head_b...  7.69 us
    pallas_call x2, Pallas kernels, project(): pl.pallas_call(columns_kernel, in_specs=[whole(None, pltpu.SMEM)] + [in_v...  7.63 us
    all_to_all x1, starting transfers between devices, local(): lax.all_to_all(pair, 'sp', split_axis=0, concat_axis=0, tiled=True)  7.6 us
  transfers between devices with their start and end apart: 12, of which 5 were waited for; matrix products, arithmetic and copies ran while one was open for 2% of the time, Pallas kernels for 9%

profile of v4, /device:TPU:1, one launch (start us, length us, event | category | flops | bytes accessed | tf_op | source)
XLA Modules:
  0.0 250.6 jit_solution(12041276043978375693)
XLA Ops:
  0.0 3.6 %collective-permute-start.8 = (bf16[2048,512]{1,0:T(8,128)(2,1)}, bf16[2048,512]{1,0:T(8,128)(2,1)}, u32[]{:S(2)}, u32[]{:S(2)}) collective-permute-start(bf16[2048,512]{1,0:T(8,128)(2,1)} %refs_4_.1), channel_id=1, source_target_pairs={{0,6},{1,7},{2,0},{3,1},{4,2},{5,3},{6,4},{7,5},{8,14},{9,15},{10,... | collective-permute-start | bytes 6291464 | tf_op jit(solution)/shard_map/ppermute | solution.py:312
  3.6 1.1 constant_dynamic-slice_fusion
  4.8 1.7 collective-permute-start.2
  6.5 2.4 pair.1
  8.9 7.6 %all-to-all-start = ((bf16[16,272,128]{2,1,0:T(8,128)(2,1)}), bf16[16,272,128]{2,1,0:T(8,128)(2,1)S(1)}, u32[]{:S(2)}, u32[]{:S(2)}) async-start(bf16[16,272,128]{2,1,0:T(8,128)(2,1)} %pair.1), calls=%async_computation | async-start | bytes 2228224 | tf_op jit(solution)/shard_map/all_to_all | solution.py:346
  16.5 0.1 copy.16
  16.6 0.1 eq.41
  16.7 0.1 eq.45
  16.8 0.1 copy.15
  16.9 0.1 mul.47
  17.1 0.1 copy.18
  17.2 0.1 copy.20
  17.3 0.1 reshape.107.weight_ref
  17.4 0.2 fusion.1
  17.7 0.1 add_add_fusion
  17.8 0.2 fusion
  18.0 14.4 %all-to-all-done.tail_ref.pair_ref = bf16[16,272,128]{2,1,0:T(8,128)(2,1)S(1)} async-done(((bf16[16,272,128]{2,1,0:T(8,128)(2,1)}), bf16[16,272,128]{2,1,0:T(8,128)(2,1)S(1)}, u32[]{:S(2)}, u32[]{:S(2)}) %all-to-all-start) | async-done | bytes 1114144 | tf_op jit(solution)/shard_map/all_to_all | solution.py:346
  32.4 3.4 %state.1 = bf16[16,128,128]{2,1,0:T(8,128)(2,1)} custom-call(bf16[16,272,128]{2,1,0:T(8,128)(2,1)S(1)} %all-to-all-done.tail_ref.pair_ref, f32[1,128]{1,0:T(1,128)S(1)} %bitcast.50), custom_call_target="tpu_custom_call" | custom-call | flops 1000000000 | bytes 2000000 | tf_op jit(solution)/shard_map/state/pallas_call | solution.py:348
  35.8 5.0 %all-to-all-start.1 = ((bf16[16,128,128]{2,1,0:T(8,128)(2,1)}), bf16[16,128,128]{2,1,0:T(8,128)(2,1)S(1)}, u32[]{:S(2)}, u32[]{:S(2)}) async-start(bf16[16,128,128]{2,1,0:T(8,128)(2,1)} %state.1), calls=%async_computation.1 | async-start | bytes 1048576 | tf_op jit(solution)/shard_map/all_to_all | solution.py:357
  40.8 2.4 scatter_custom_fusion.slot_ref
  43.3 18.4 %collective-permute-done.2.refs_0_ = bf16[512,512]{1,0:T(8,128)(2,1)} collective-permute-done((bf16[512,512]{1,0:T(8,128)(2,1)S(1)}, bf16[512,512]{1,0:T(8,128)(2,1)}, u32[]{:S(2)}, u32[]{:S(2)}) %collective-permute-start.2) | collective-permute-done | bytes 524320 | tf_op jit(solution)/shard_map/ppermute | solution.py:312
  61.6 1.6 collective-permute-start.5
  63.3 2.5 collective-permute-start.4
  65.8 7.7 %within.1 = (f32[128,2048]{1,0:T(8,128)}, bf16[128,2048]{1,0:T(8,128)(2,1)}, bf16[128,2048]{1,0:T(8,128)(2,1)}) custom-call(bf16[128,2048]{1,0:T(8,128)(2,1)} %bitcast.60, bf16[128,2048]{1,0:T(8,128)(2,1)} %bitcast.55, bf16[128,2048]{1,0:T(8,128)(2,1)} %bitcast.57, bf16[16,272,128]{2,1,0:T(8,128)(2,1)} %copy-done.6), custom_call_target="tpu_custom_call" | custom-call | flops 2000000000 | bytes 3000000 | tf_op jit(solution)/shard_map/within/pallas_call | solution.py:365
  73.5 1.2 copy-done
  74.7 1.0 copy-done.4
  75.8 1.0 copy-done.5
  76.8 0.6 finish.2.mine_b
  77.4 1.0 copy-done.3
  78.5 0.6 finish.3.mine_a
  79.1 2.5 collective-permute-start.1
  81.6 0.1 collective-permute-start
  81.7 0.1 pad_add_fusion.place_ref
  81.8 1.0 collective-permute-done.1.other_b
  82.8 0.4 collective-permute-done.other_a
  83.2 4.0 %shard_map.136 = (bf16[128,1024]{1,0:T(8,128)(2,1)S(1)}, bf16[128,1024]{1,0:T(8,128)(2,1)}) custom-call(s32[4]{0:T(128)S(1)} %pad_add_fusion.place_ref, bf16[128,1024]{1,0:T(8,128)(2,1)S(1)} %finish.3.mine_a, bf16[128,1024]{1,0:T(8,128)(2,1)S(1)} %finish.2.mine_b, bf16[128,1024]{1,0:T(8,128)(2,1)S(1)} %collective-permute-done.other_a, ...), custom_call_target="tpu_custom_call" | custom-call | flops 1073741824 | bytes 4194304 | tf_op jit(solution)/shard_map/pallas_call | solution.py:401
  87.2 0.5 collective-permute-start.6
  87.7 3.6 %shard_map.137 = (bf16[128,1024]{1,0:T(8,128)(2,1)S(1)}, bf16[128,1024]{1,0:T(8,128)(2,1)S(1)}) custom-call(s32[4]{0:T(128)S(1)} %pad_add_fusion.place_ref, bf16[128,1024]{1,0:T(8,128)(2,1)S(1)} %finish.3.mine_a, bf16[128,1024]{1,0:T(8,128)(2,1)S(1)} %finish.2.mine_b, bf16[128,1024]{1,0:T(8,128)(2,1)S(1)} %collective-permute-done.other_a, ...), custom_call_target="tpu_custom_call" | custom-call | flops 1073741824 | bytes 4194304 | tf_op jit(solution)/shard_map/pallas_call | solution.py:401
  91.3 0.2 collective-permute-start.9
  91.5 0.1 stack.50.order_ref
  91.6 1.3 collective-permute-done.9.refs_3_
  92.9 1.2 copy-done.7
  94.1 2.9 %route.1 = (bf16[640,32,128]{2,1,0:T(8,128)(2,1)S(1)}, bf16[128,32,128]{2,1,0:T(8,128)(2,1)S(1)}) custom-call(s32[640]{0:T(1024)S(1)} %scatter_custom_fusion.slot_ref, s32[8]{0:T(128)S(1)} %stack.50.order_ref, bf16[128,1024]{1,0:T(8,128)(2,1)S(1)} %get-tuple-element.25.refs_0_, bf16[128,1024]{1,0:T(8,128)(2,1)S(1)} %collective-permute-done.6.refs_1_, ...), custom_call_target="tpu_custom_call" | custom-call | flops 40000000 | bytes 12000000 | tf_op jit(solution)/shard_map/route/pallas_call | solution.py:430
  97.0 0.0 copy-start.12
  97.0 71.8 %all_to_all.20 = bf16[128,160,128]{2,1,0:T(8,128)(2,1)S(1)} all-to-all(bf16[128,160,128]{2,1,0:T(8,128)(2,1)S(1)} %bitcast.40), channel_id=1, replica_groups=mesh['sp'=16,'dp'=8] {'sp','dp'}, dimensions={0} | all-to-all | bytes 10485760 | tf_op jit(solution)/shard_map/all_to_all | solution.py:459
  168.8 10.5 %expert.1 = bf16[640,32,128]{2,1,0:T(8,128)(2,1)S(1)} custom-call(bf16[640,32,128]{2,1,0:T(8,128)(2,1)S(1)} %bitcast.41, bf16[4096,512]{1,0:T(8,128)(2,1)S(1)} %bitcast.51, bf16[4096,512]{1,0:T(8,128)(2,1)S(1)} %bitcast.52, bf16[512,4096]{1,0:T(8,128)(2,1)S(1)} %bitcast.53), custom_call_target="tpu_custom_call" | custom-call | flops 8000000000 | bytes 24000000 | tf_op jit(solution)/shard_map/expert/pallas_call | solution.py:462
  179.4 68.2 %all_to_all.21 = bf16[128,160,128]{2,1,0:T(8,128)(2,1)S(1)} all-to-all(bf16[128,160,128]{2,1,0:T(8,128)(2,1)S(1)} %bitcast.42), channel_id=1, replica_groups=mesh['sp'=16,'dp'=8] {'sp','dp'}, dimensions={0} | all-to-all | bytes 10485760 | tf_op jit(solution)/shard_map/all_to_all | solution.py:480
  247.6 3.0 %combine.1 = bf16[128,4096]{1,0:T(8,128)(2,1)} custom-call(s32[512]{0:T(512)S(1)} %multiply_add_fusion.target_ref, f32[512]{0:T(512)S(1)} %reshape.107.weight_ref, bf16[640,32,128]{2,1,0:T(8,128)(2,1)S(1)} %bitcast.39, bf16[128,32,128]{2,1,0:T(8,128)(2,1)S(1)} %get-tuple-element.30.hidden_ref), custom_call_target="tpu_custom_call" | custom-call | flops 400000000 | bytes 8000000 | tf_op jit(solution)/shard_map/combine/pallas_call | solution.py:481
  (43 shorter events, 0.2 us)
Async XLA Ops:
  0.0 32.4 %copy-start.10 = (f32[128]{0:T(128)S(1)}, f32[128]{0:T(128)}, u32[]{:S(2)}) copy-start(f32[128]{0:T(128)} %param.18) | copy-start | bytes 1540
  0.0 16.5 %copy-start.14 = (s32[1,128,4]{1,2,0:T(4,128)S(1)}, s32[1,128,4]{1,2,0:T(4,128)}, u32[]{:S(2)}) copy-start(s32[1,128,4]{1,2,0:T(4,128)} %param.23) | copy-start | bytes 6148
  0.0 17.2 %copy-start.15 = (f32[1,128,4]{1,2,0:T(4,128)S(1)}, f32[1,128,4]{1,2,0:T(4,128)}, u32[]{:S(2)}) copy-start(f32[1,128,4]{1,2,0:T(4,128)} %param.24) | copy-start | bytes 6148
  0.0 87.7 %collective-permute-start.8 = (bf16[2048,512]{1,0:T(8,128)(2,1)}, bf16[2048,512]{1,0:T(8,128)(2,1)}, u32[]{:S(2)}, u32[]{:S(2)}) collective-permute-start(bf16[2048,512]{1,0:T(8,128)(2,1)} %refs_4_.1), channel_id=1, source_target_pairs={{0,6},{1,7},{2,0},{3,1},{4,2},{5,3},{6,4},{7,5},{8,14},{9,15},{10,... | collective-permute-start | bytes 6291464 | tf_op jit(solution)/shard_map/ppermute | solution.py:312
  3.6 84.1 %collective-permute-start.7 = (bf16[2048,512]{1,0:T(8,128)(2,1)}, bf16[2048,512]{1,0:T(8,128)(2,1)}, u32[]{:S(2)}, u32[]{:S(2)}) collective-permute-start(bf16[2048,512]{1,0:T(8,128)(2,1)} %refs_4_.1), channel_id=1, source_target_pairs={{0,2},{1,3},{2,4},{3,5},{4,6},{5,7},{6,0},{7,1},{8,10},{9,11},{10,... | collective-permute-start | bytes 6291464 | tf_op jit(solution)/shard_map/ppermute | solution.py:312
  4.8 56.9 %collective-permute-start.2 = (bf16[512,512]{1,0:T(8,128)(2,1)S(1)}, bf16[512,512]{1,0:T(8,128)(2,1)}, u32[]{:S(2)}, u32[]{:S(2)}) collective-permute-start(bf16[512,512]{1,0:T(8,128)(2,1)S(1)} %constant_dynamic-slice_fusion), channel_id=1, source_target_pairs={{0,4},{1,5},{2,6},{3,7},{4,0},{5,1},{6,2},{7,3},{8,12},{9,13},{10,... | collective-permute-start | bytes 1572872 | tf_op jit(solution)/shard_map/ppermute | solution.py:312
  8.9 23.5 %all-to-all-start = ((bf16[16,272,128]{2,1,0:T(8,128)(2,1)}), bf16[16,272,128]{2,1,0:T(8,128)(2,1)S(1)}, u32[]{:S(2)}, u32[]{:S(2)}) async-start(bf16[16,272,128]{2,1,0:T(8,128)(2,1)} %pair.1), calls=%async_computation | async-start | bytes 2228224 | tf_op jit(solution)/shard_map/all_to_all | solution.py:346
  32.4 3.4 %copy-start.6 = (bf16[16,272,128]{2,1,0:T(8,128)(2,1)}, bf16[16,272,128]{2,1,0:T(8,128)(2,1)S(1)}, u32[]{:S(2)}) copy-start(bf16[16,272,128]{2,1,0:T(8,128)(2,1)S(1)} %all-to-all-done.tail_ref.pair_ref) | copy-start | bytes 3342340
  35.8 37.7 %copy-start.2 = (bf16[1,128,2048]{2,1,0:T(8,128)(2,1)S(1)}, bf16[1,128,2048]{2,1,0:T(8,128)(2,1)}, u32[]{:S(2)}) copy-start(bf16[1,128,2048]{2,1,0:T(8,128)(2,1)} %param.17) | copy-start | bytes 1572868
  35.8 37.7 %copy-start.9 = (f32[128]{0:T(128)S(1)}, f32[128]{0:T(128)}, u32[]{:S(2)}) copy-start(f32[128]{0:T(128)} %param.19) | copy-start | bytes 1540
  35.8 37.7 %all-to-all-start.1 = ((bf16[16,128,128]{2,1,0:T(8,128)(2,1)}), bf16[16,128,128]{2,1,0:T(8,128)(2,1)S(1)}, u32[]{:S(2)}, u32[]{:S(2)}) async-start(bf16[16,128,128]{2,1,0:T(8,128)(2,1)} %state.1), calls=%async_computation.1 | async-start | bytes 1048576 | tf_op jit(solution)/shard_map/all_to_all | solution.py:357
  61.6 17.5 %collective-permute-start.5 = (bf16[512,512]{1,0:T(8,128)(2,1)}, bf16[512,512]{1,0:T(8,128)(2,1)}, u32[]{:S(2)}, u32[]{:S(2)}) collective-permute-start(bf16[512,512]{1,0:T(8,128)(2,1)} %collective-permute-done.2.refs_0_), channel_id=1, source_target_pairs={{0,32},{8,40},{16,48},{24,56},{32,64},{40,72},{48,80},{56,88},{64,... | collective-permute-start | bytes 1572872 | tf_op jit(solution)/shard_map/ppermute | solution.py:320
  63.3 18.3 %collective-permute-start.4 = (bf16[512,512]{1,0:T(8,128)(2,1)}, bf16[512,512]{1,0:T(8,128)(2,1)}, u32[]{:S(2)}, u32[]{:S(2)}) collective-permute-start(bf16[512,512]{1,0:T(8,128)(2,1)} %collective-permute-done.2.refs_0_), channel_id=1, source_target_pairs={{0,24},{8,0},{16,8},{24,16},{32,56},{40,32},{48,40},{56,48},{64,88... | collective-permute-start | bytes 1572872 | tf_op jit(solution)/shard_map/ppermute | solution.py:316
  65.8 16.0 %collective-permute-start.3 = (bf16[512,512]{1,0:T(8,128)(2,1)}, bf16[512,512]{1,0:T(8,128)(2,1)}, u32[]{:S(2)}, u32[]{:S(2)}) collective-permute-start(bf16[512,512]{1,0:T(8,128)(2,1)} %collective-permute-done.2.refs_0_), channel_id=1, source_target_pairs={{0,8},{8,16},{16,24},{24,0},{32,40},{40,48},{48,56},{56,32},{64,72... | collective-permute-start | bytes 1572872 | tf_op jit(solution)/shard_map/ppermute | solution.py:316
  65.8 17.4 %copy-start.1 = (bf16[2048,512]{1,0:T(8,128)(2,1)S(1)}, bf16[2048,512]{1,0:T(8,128)(2,1)}, u32[]{:S(2)}) copy-start(bf16[2048,512]{1,0:T(8,128)(2,1)} %refs_4_.1) | copy-start | bytes 6291460
  73.5 1.2 copy-start
  74.7 1.0 copy-start.4
  75.8 1.0 copy-start.5
  77.4 1.0 copy-start.3
  79.1 3.7 %collective-permute-start.1 = (bf16[128,1024]{1,0:T(8,128)(2,1)S(1)}, bf16[128,1024]{1,0:T(8,128)(2,1)S(1)}, u32[]{:S(2)}, u32[]{:S(2)}) collective-permute-start(bf16[128,1024]{1,0:T(8,128)(2,1)S(1)} %finish.2.mine_b), channel_id=1, source_target_pairs={{0,1},{1,0},{2,3},{3,2},{4,5},{5,4},{6,7},{7,6},{8,9},{9,8},{10,11... | collective-permute-start | bytes 786440 | tf_op jit(solution)/shard_map/ppermute | solution.py:328
  81.6 1.5 collective-permute-start
  81.8 11.1 %copy-start.8 = (f32[4096]{0:T(1024)S(1)}, f32[4096]{0:T(1024)}, u32[]{:S(2)}) copy-start(f32[4096]{0:T(1024)} %param.22) | copy-start | bytes 49156
  87.2 4.4 %collective-permute-start.6 = (bf16[128,1024]{1,0:T(8,128)(2,1)}, bf16[128,1024]{1,0:T(8,128)(2,1)S(1)}, u32[]{:S(2)}, u32[]{:S(2)}) collective-permute-start(bf16[128,1024]{1,0:T(8,128)(2,1)} %get-tuple-element.26), channel_id=1, source_target_pairs={{0,1},{1,0},{2,3},{3,2},{4,5},{5,4},{6,7},{7,6},{8,9},{9,8},{10,11... | collective-permute-start | bytes 786440 | tf_op jit(solution)/shard_map/ppermute | solution.py:328
  91.3 1.6 collective-permute-start.9
  92.9 1.2 copy-start.7
  94.1 74.7 %copy-start.13 = (bf16[1,512,4096]{2,1,0:T(8,128)(2,1)S(1)}, bf16[1,512,4096]{2,1,0:T(8,128)(2,1)}, u32[]{:S(2)}) copy-start(bf16[1,512,4096]{2,1,0:T(8,128)(2,1)} %param.27) | copy-start | bytes 12582916
  97.0 71.8 %copy-start.11 = (bf16[1,4096,512]{2,1,0:T(8,128)(2,1)S(1)}, bf16[1,4096,512]{2,1,0:T(8,128)(2,1)}, u32[]{:S(2)}) copy-start(bf16[1,4096,512]{2,1,0:T(8,128)(2,1)} %param.25) | copy-start | bytes 12582916
  97.0 71.8 %copy-start.12 = (bf16[1,4096,512]{2,1,0:T(8,128)(2,1)S(1)}, bf16[1,4096,512]{2,1,0:T(8,128)(2,1)}, u32[]{:S(2)}) copy-start(bf16[1,4096,512]{2,1,0:T(8,128)(2,1)} %param.26) | copy-start | bytes 12582916

commit v5 on v4

--- a/solution.py
+++ b/solution.py
@@ -437,8 +437,8 @@
         ],
         scratch_shapes=[
             pltpu.VMEM((tokens, width), F32),
-            pltpu.VMEM((skew * pieces, LANES), F32),
-            pltpu.VMEM((skew * pieces, LANES), F32),
+            pltpu.VMEM((skew * pieces + 8, LANES), F32),
+            pltpu.VMEM((skew * pieces + 8, LANES), F32),
         ],
         cost_estimate=cost(4e7, 12e6),
         compiler_params=pltpu.CompilerParams(vmem_limit_bytes=24 * 2**20),
@@ -465,7 +465,7 @@
         out_specs=in_vmem,
         out_shape=jax.ShapeDtypeStruct((slots, pieces, LANES), BF16),
         scratch_shapes=[
-            pltpu.VMEM(((rows + 1) * pieces, LANES), F32),
+            pltpu.VMEM(((rows + 1) * pieces + 8, LANES), F32),
             pltpu.VMEM((rows, width), BF16),
         ],
         cost_estimate=cost(8e9, 24e6),
@@ -488,7 +488,7 @@
         ],
         out_specs=whole(None, pltpu.VMEM),
         out_shape=jax.ShapeDtypeStruct((tokens, width), BF16),
-        scratch_shapes=[pltpu.VMEM((skew * pieces, LANES), F32)],
+        scratch_shapes=[pltpu.VMEM((skew * pieces + 8, LANES), F32)],
         cost_estimate=cost(4e8, 8e6),
         compiler_params=pltpu.CompilerParams(vmem_limit_bytes=16 * 2**20),
         name="combine",

time: 251 us -> 251 us (level)
  no operation moved by 1% of the time
where the time goes in v5:
time: 251 us
  blocking collectives  140 us (56%)
  Pallas kernels  38.8 us (15%)
  waiting for transfers between devices  35.4 us (14%)
  starting transfers between devices  25.3 us (10%)
  local copies, waits for them, and re-layouts  10.2 us (4%)
    all_to_all x1, blocking collectives, local(): rows_in = exchange(outgoing.reshape(chunk)).reshape(slots, pieces, LANES)  71.8 us
    all_to_all x1, blocking collectives, local(): back = exchange(results.reshape(chunk)).reshape(slots, pieces, LANES)  68.2 us
    ppermute x3, waiting for transfers between devices, hop(): lax.ppermute(x, 'dp', [(d, (d + 2 * chips) % ring) for d in range(ring)])  18.4 us
    all_to_all x1, waiting for transfers between devices, local(): lax.all_to_all(pair, 'sp', split_axis=0, concat_axis=0, tiled=True)  14.4 us
    pallas_call x1, Pallas kernels, local(): pl.pallas_call(expert_kernel, in_specs=[in_vmem] * 4, out_specs=in_vmem,...  10.6 us
    pallas_call x1, Pallas kernels, local(): pl.pallas_call(within_kernel, grid=(heads // per_step,), in_specs=[head_b...  7.69 us
    pallas_call x2, Pallas kernels, project(): pl.pallas_call(columns_kernel, in_specs=[whole(None, pltpu.SMEM)] + [in_v...  7.63 us
    all_to_all x1, starting transfers between devices, local(): lax.all_to_all(pair, 'sp', split_axis=0, concat_axis=0, tiled=True)  7.6 us
  transfers between devices with their start and end apart: 12, of which 5 were waited for; matrix products, arithmetic and copies ran while one was open for 2% of the time, Pallas kernels for 9%

profile of v5, /device:TPU:1, one launch (start us, length us, event | category | flops | bytes accessed | tf_op | source)
XLA Modules:
  0.0 250.6 jit_solution(14703281518830628323)
XLA Ops:
  0.0 3.6 %collective-permute-start.8 = (bf16[2048,512]{1,0:T(8,128)(2,1)}, bf16[2048,512]{1,0:T(8,128)(2,1)}, u32[]{:S(2)}, u32[]{:S(2)}) collective-permute-start(bf16[2048,512]{1,0:T(8,128)(2,1)} %refs_4_.1), channel_id=1, source_target_pairs={{0,6},{1,7},{2,0},{3,1},{4,2},{5,3},{6,4},{7,5},{8,14},{9,15},{10,... | collective-permute-start | bytes 6291464 | tf_op jit(solution)/shard_map/ppermute | solution.py:312
  3.6 1.1 constant_dynamic-slice_fusion
  4.8 1.7 collective-permute-start.2
  6.5 2.4 pair.1
  8.9 7.6 %all-to-all-start = ((bf16[16,272,128]{2,1,0:T(8,128)(2,1)}), bf16[16,272,128]{2,1,0:T(8,128)(2,1)S(1)}, u32[]{:S(2)}, u32[]{:S(2)}) async-start(bf16[16,272,128]{2,1,0:T(8,128)(2,1)} %pair.1), calls=%async_computation | async-start | bytes 2228224 | tf_op jit(solution)/shard_map/all_to_all | solution.py:346
  16.5 0.1 copy.16
  16.6 0.1 eq.41
  16.7 0.1 eq.45
  16.8 0.1 copy.15
  16.9 0.1 mul.47
  17.1 0.1 copy.18
  17.2 0.1 copy.20
  17.3 0.1 reshape.107.weight_ref
  17.4 0.2 fusion.1
  17.7 0.1 add_add_fusion
  17.8 0.2 fusion
  18.0 14.4 %all-to-all-done.tail_ref.pair_ref = bf16[16,272,128]{2,1,0:T(8,128)(2,1)S(1)} async-done(((bf16[16,272,128]{2,1,0:T(8,128)(2,1)}), bf16[16,272,128]{2,1,0:T(8,128)(2,1)S(1)}, u32[]{:S(2)}, u32[]{:S(2)}) %all-to-all-start) | async-done | bytes 1114144 | tf_op jit(solution)/shard_map/all_to_all | solution.py:346
  32.4 3.4 %state.1 = bf16[16,128,128]{2,1,0:T(8,128)(2,1)} custom-call(bf16[16,272,128]{2,1,0:T(8,128)(2,1)S(1)} %all-to-all-done.tail_ref.pair_ref, f32[1,128]{1,0:T(1,128)S(1)} %bitcast.50), custom_call_target="tpu_custom_call" | custom-call | flops 1000000000 | bytes 2000000 | tf_op jit(solution)/shard_map/state/pallas_call | solution.py:348
  35.8 5.0 %all-to-all-start.1 = ((bf16[16,128,128]{2,1,0:T(8,128)(2,1)}), bf16[16,128,128]{2,1,0:T(8,128)(2,1)S(1)}, u32[]{:S(2)}, u32[]{:S(2)}) async-start(bf16[16,128,128]{2,1,0:T(8,128)(2,1)} %state.1), calls=%async_computation.1 | async-start | bytes 1048576 | tf_op jit(solution)/shard_map/all_to_all | solution.py:357
  40.8 2.4 scatter_custom_fusion.slot_ref
  43.3 18.4 %collective-permute-done.2.refs_0_ = bf16[512,512]{1,0:T(8,128)(2,1)} collective-permute-done((bf16[512,512]{1,0:T(8,128)(2,1)S(1)}, bf16[512,512]{1,0:T(8,128)(2,1)}, u32[]{:S(2)}, u32[]{:S(2)}) %collective-permute-start.2) | collective-permute-done | bytes 524320 | tf_op jit(solution)/shard_map/ppermute | solution.py:312
  61.6 1.6 collective-permute-start.5
  63.3 2.5 collective-permute-start.4
  65.8 7.7 %within.1 = (f32[128,2048]{1,0:T(8,128)}, bf16[128,2048]{1,0:T(8,128)(2,1)}, bf16[128,2048]{1,0:T(8,128)(2,1)}) custom-call(bf16[128,2048]{1,0:T(8,128)(2,1)} %bitcast.60, bf16[128,2048]{1,0:T(8,128)(2,1)} %bitcast.55, bf16[128,2048]{1,0:T(8,128)(2,1)} %bitcast.57, bf16[16,272,128]{2,1,0:T(8,128)(2,1)} %copy-done.6), custom_call_target="tpu_custom_call" | custom-call | flops 2000000000 | bytes 3000000 | tf_op jit(solution)/shard_map/within/pallas_call | solution.py:365
  73.5 1.2 copy-done
  74.7 1.0 copy-done.4
  75.8 1.0 copy-done.5
  76.8 0.6 finish.2.mine_b
  77.4 1.0 copy-done.3
  78.5 0.6 finish.3.mine_a
  79.1 2.5 collective-permute-start.1
  81.6 0.1 collective-permute-start
  81.7 0.1 pad_add_fusion.place_ref
  81.8 1.0 collective-permute-done.1.other_b
  82.8 0.4 collective-permute-done.other_a
  83.2 4.0 %shard_map.136 = (bf16[128,1024]{1,0:T(8,128)(2,1)S(1)}, bf16[128,1024]{1,0:T(8,128)(2,1)}) custom-call(s32[4]{0:T(128)S(1)} %pad_add_fusion.place_ref, bf16[128,1024]{1,0:T(8,128)(2,1)S(1)} %finish.3.mine_a, bf16[128,1024]{1,0:T(8,128)(2,1)S(1)} %finish.2.mine_b, bf16[128,1024]{1,0:T(8,128)(2,1)S(1)} %collective-permute-done.other_a, ...), custom_call_target="tpu_custom_call" | custom-call | flops 1073741824 | bytes 4194304 | tf_op jit(solution)/shard_map/pallas_call | solution.py:401
  87.2 0.5 collective-permute-start.6
  87.7 3.6 %shard_map.137 = (bf16[128,1024]{1,0:T(8,128)(2,1)S(1)}, bf16[128,1024]{1,0:T(8,128)(2,1)S(1)}) custom-call(s32[4]{0:T(128)S(1)} %pad_add_fusion.place_ref, bf16[128,1024]{1,0:T(8,128)(2,1)S(1)} %finish.3.mine_a, bf16[128,1024]{1,0:T(8,128)(2,1)S(1)} %finish.2.mine_b, bf16[128,1024]{1,0:T(8,128)(2,1)S(1)} %collective-permute-done.other_a, ...), custom_call_target="tpu_custom_call" | custom-call | flops 1073741824 | bytes 4194304 | tf_op jit(solution)/shard_map/pallas_call | solution.py:401
  91.3 0.2 collective-permute-start.9
  91.5 0.1 stack.50.order_ref
  91.6 1.3 collective-permute-done.9.refs_3_
  92.9 1.2 copy-done.7
  94.1 2.9 %route.1 = (bf16[640,32,128]{2,1,0:T(8,128)(2,1)S(1)}, bf16[128,32,128]{2,1,0:T(8,128)(2,1)S(1)}) custom-call(s32[640]{0:T(1024)S(1)} %scatter_custom_fusion.slot_ref, s32[8]{0:T(128)S(1)} %stack.50.order_ref, bf16[128,1024]{1,0:T(8,128)(2,1)S(1)} %get-tuple-element.25.refs_0_, bf16[128,1024]{1,0:T(8,128)(2,1)S(1)} %collective-permute-done.6.refs_1_, ...), custom_call_target="tpu_custom_call" | custom-call | flops 40000000 | bytes 12000000 | tf_op jit(solution)/shard_map/route/pallas_call | solution.py:430
  97.0 0.0 copy-start.11
  97.0 71.8 %all_to_all.20 = bf16[128,160,128]{2,1,0:T(8,128)(2,1)S(1)} all-to-all(bf16[128,160,128]{2,1,0:T(8,128)(2,1)S(1)} %bitcast.40), channel_id=1, replica_groups=mesh['sp'=16,'dp'=8] {'sp','dp'}, dimensions={0} | all-to-all | bytes 10485760 | tf_op jit(solution)/shard_map/all_to_all | solution.py:459
  168.8 10.6 %expert.1 = bf16[640,32,128]{2,1,0:T(8,128)(2,1)S(1)} custom-call(bf16[640,32,128]{2,1,0:T(8,128)(2,1)S(1)} %bitcast.41, bf16[4096,512]{1,0:T(8,128)(2,1)S(1)} %bitcast.51, bf16[4096,512]{1,0:T(8,128)(2,1)S(1)} %bitcast.52, bf16[512,4096]{1,0:T(8,128)(2,1)S(1)} %bitcast.53), custom_call_target="tpu_custom_call" | custom-call | flops 8000000000 | bytes 24000000 | tf_op jit(solution)/shard_map/expert/pallas_call | solution.py:462
  179.4 68.2 %all_to_all.21 = bf16[128,160,128]{2,1,0:T(8,128)(2,1)S(1)} all-to-all(bf16[128,160,128]{2,1,0:T(8,128)(2,1)S(1)} %bitcast.42), channel_id=1, replica_groups=mesh['sp'=16,'dp'=8] {'sp','dp'}, dimensions={0} | all-to-all | bytes 10485760 | tf_op jit(solution)/shard_map/all_to_all | solution.py:480
  247.6 3.0 %combine.1 = bf16[128,4096]{1,0:T(8,128)(2,1)} custom-call(s32[512]{0:T(512)S(1)} %multiply_add_fusion.target_ref, f32[512]{0:T(512)S(1)} %reshape.107.weight_ref, bf16[640,32,128]{2,1,0:T(8,128)(2,1)S(1)} %bitcast.39, bf16[128,32,128]{2,1,0:T(8,128)(2,1)S(1)} %get-tuple-element.30.hidden_ref), custom_call_target="tpu_custom_call" | custom-call | flops 400000000 | bytes 8000000 | tf_op jit(solution)/shard_map/combine/pallas_call | solution.py:481
  (43 shorter events, 0.2 us)
Async XLA Ops:
  0.0 32.4 %copy-start.10 = (f32[128]{0:T(128)S(1)}, f32[128]{0:T(128)}, u32[]{:S(2)}) copy-start(f32[128]{0:T(128)} %param.18) | copy-start | bytes 1540
  0.0 16.5 %copy-start.14 = (s32[1,128,4]{1,2,0:T(4,128)S(1)}, s32[1,128,4]{1,2,0:T(4,128)}, u32[]{:S(2)}) copy-start(s32[1,128,4]{1,2,0:T(4,128)} %param.23) | copy-start | bytes 6148
  0.0 17.2 %copy-start.15 = (f32[1,128,4]{1,2,0:T(4,128)S(1)}, f32[1,128,4]{1,2,0:T(4,128)}, u32[]{:S(2)}) copy-start(f32[1,128,4]{1,2,0:T(4,128)} %param.24) | copy-start | bytes 6148
  0.0 87.7 %collective-permute-start.8 = (bf16[2048,512]{1,0:T(8,128)(2,1)}, bf16[2048,512]{1,0:T(8,128)(2,1)}, u32[]{:S(2)}, u32[]{:S(2)}) collective-permute-start(bf16[2048,512]{1,0:T(8,128)(2,1)} %refs_4_.1), channel_id=1, source_target_pairs={{0,6},{1,7},{2,0},{3,1},{4,2},{5,3},{6,4},{7,5},{8,14},{9,15},{10,... | collective-permute-start | bytes 6291464 | tf_op jit(solution)/shard_map/ppermute | solution.py:312
  3.6 84.1 %collective-permute-start.7 = (bf16[2048,512]{1,0:T(8,128)(2,1)}, bf16[2048,512]{1,0:T(8,128)(2,1)}, u32[]{:S(2)}, u32[]{:S(2)}) collective-permute-start(bf16[2048,512]{1,0:T(8,128)(2,1)} %refs_4_.1), channel_id=1, source_target_pairs={{0,2},{1,3},{2,4},{3,5},{4,6},{5,7},{6,0},{7,1},{8,10},{9,11},{10,... | collective-permute-start | bytes 6291464 | tf_op jit(solution)/shard_map/ppermute | solution.py:312
  4.8 56.9 %collective-permute-start.2 = (bf16[512,512]{1,0:T(8,128)(2,1)S(1)}, bf16[512,512]{1,0:T(8,128)(2,1)}, u32[]{:S(2)}, u32[]{:S(2)}) collective-permute-start(bf16[512,512]{1,0:T(8,128)(2,1)S(1)} %constant_dynamic-slice_fusion), channel_id=1, source_target_pairs={{0,4},{1,5},{2,6},{3,7},{4,0},{5,1},{6,2},{7,3},{8,12},{9,13},{10,... | collective-permute-start | bytes 1572872 | tf_op jit(solution)/shard_map/ppermute | solution.py:312
  8.9 23.5 %all-to-all-start = ((bf16[16,272,128]{2,1,0:T(8,128)(2,1)}), bf16[16,272,128]{2,1,0:T(8,128)(2,1)S(1)}, u32[]{:S(2)}, u32[]{:S(2)}) async-start(bf16[16,272,128]{2,1,0:T(8,128)(2,1)} %pair.1), calls=%async_computation | async-start | bytes 2228224 | tf_op jit(solution)/shard_map/all_to_all | solution.py:346
  32.4 3.4 %copy-start.6 = (bf16[16,272,128]{2,1,0:T(8,128)(2,1)}, bf16[16,272,128]{2,1,0:T(8,128)(2,1)S(1)}, u32[]{:S(2)}) copy-start(bf16[16,272,128]{2,1,0:T(8,128)(2,1)S(1)} %all-to-all-done.tail_ref.pair_ref) | copy-start | bytes 3342340
  35.8 37.7 %copy-start.2 = (bf16[1,128,2048]{2,1,0:T(8,128)(2,1)S(1)}, bf16[1,128,2048]{2,1,0:T(8,128)(2,1)}, u32[]{:S(2)}) copy-start(bf16[1,128,2048]{2,1,0:T(8,128)(2,1)} %param.17) | copy-start | bytes 1572868
  35.8 37.7 %copy-start.9 = (f32[128]{0:T(128)S(1)}, f32[128]{0:T(128)}, u32[]{:S(2)}) copy-start(f32[128]{0:T(128)} %param.19) | copy-start | bytes 1540
  35.8 37.7 %all-to-all-start.1 = ((bf16[16,128,128]{2,1,0:T(8,128)(2,1)}), bf16[16,128,128]{2,1,0:T(8,128)(2,1)S(1)}, u32[]{:S(2)}, u32[]{:S(2)}) async-start(bf16[16,128,128]{2,1,0:T(8,128)(2,1)} %state.1), calls=%async_computation.1 | async-start | bytes 1048576 | tf_op jit(solution)/shard_map/all_to_all | solution.py:357
  61.6 17.5 %collective-permute-start.5 = (bf16[512,512]{1,0:T(8,128)(2,1)}, bf16[512,512]{1,0:T(8,128)(2,1)}, u32[]{:S(2)}, u32[]{:S(2)}) collective-permute-start(bf16[512,512]{1,0:T(8,128)(2,1)} %collective-permute-done.2.refs_0_), channel_id=1, source_target_pairs={{0,32},{8,40},{16,48},{24,56},{32,64},{40,72},{48,80},{56,88},{64,... | collective-permute-start | bytes 1572872 | tf_op jit(solution)/shard_map/ppermute | solution.py:320
  63.3 18.3 %collective-permute-start.4 = (bf16[512,512]{1,0:T(8,128)(2,1)}, bf16[512,512]{1,0:T(8,128)(2,1)}, u32[]{:S(2)}, u32[]{:S(2)}) collective-permute-start(bf16[512,512]{1,0:T(8,128)(2,1)} %collective-permute-done.2.refs_0_), channel_id=1, source_target_pairs={{0,24},{8,0},{16,8},{24,16},{32,56},{40,32},{48,40},{56,48},{64,88... | collective-permute-start | bytes 1572872 | tf_op jit(solution)/shard_map/ppermute | solution.py:316
  65.8 16.0 %collective-permute-start.3 = (bf16[512,512]{1,0:T(8,128)(2,1)}, bf16[512,512]{1,0:T(8,128)(2,1)}, u32[]{:S(2)}, u32[]{:S(2)}) collective-permute-start(bf16[512,512]{1,0:T(8,128)(2,1)} %collective-permute-done.2.refs_0_), channel_id=1, source_target_pairs={{0,8},{8,16},{16,24},{24,0},{32,40},{40,48},{48,56},{56,32},{64,72... | collective-permute-start | bytes 1572872 | tf_op jit(solution)/shard_map/ppermute | solution.py:316
  65.8 17.4 %copy-start.1 = (bf16[2048,512]{1,0:T(8,128)(2,1)S(1)}, bf16[2048,512]{1,0:T(8,128)(2,1)}, u32[]{:S(2)}) copy-start(bf16[2048,512]{1,0:T(8,128)(2,1)} %refs_4_.1) | copy-start | bytes 6291460
  73.5 1.2 copy-start
  74.7 1.0 copy-start.4
  75.8 1.0 copy-start.5
  77.4 1.0 copy-start.3
  79.1 3.7 %collective-permute-start.1 = (bf16[128,1024]{1,0:T(8,128)(2,1)S(1)}, bf16[128,1024]{1,0:T(8,128)(2,1)S(1)}, u32[]{:S(2)}, u32[]{:S(2)}) collective-permute-start(bf16[128,1024]{1,0:T(8,128)(2,1)S(1)} %finish.2.mine_b), channel_id=1, source_target_pairs={{0,1},{1,0},{2,3},{3,2},{4,5},{5,4},{6,7},{7,6},{8,9},{9,8},{10,11... | collective-permute-start | bytes 786440 | tf_op jit(solution)/shard_map/ppermute | solution.py:328
  81.6 1.5 collective-permute-start
  81.8 11.1 %copy-start.8 = (f32[4096]{0:T(1024)S(1)}, f32[4096]{0:T(1024)}, u32[]{:S(2)}) copy-start(f32[4096]{0:T(1024)} %param.22) | copy-start | bytes 49156
  87.2 4.4 %collective-permute-start.6 = (bf16[128,1024]{1,0:T(8,128)(2,1)}, bf16[128,1024]{1,0:T(8,128)(2,1)S(1)}, u32[]{:S(2)}, u32[]{:S(2)}) collective-permute-start(bf16[128,1024]{1,0:T(8,128)(2,1)} %get-tuple-element.26), channel_id=1, source_target_pairs={{0,1},{1,0},{2,3},{3,2},{4,5},{5,4},{6,7},{7,6},{8,9},{9,8},{10,11... | collective-permute-start | bytes 786440 | tf_op jit(solution)/shard_map/ppermute | solution.py:328
  91.3 1.6 collective-permute-start.9
  92.9 1.2 copy-start.7
  94.1 74.7 %copy-start.13 = (bf16[1,512,4096]{2,1,0:T(8,128)(2,1)S(1)}, bf16[1,512,4096]{2,1,0:T(8,128)(2,1)}, u32[]{:S(2)}) copy-start(bf16[1,512,4096]{2,1,0:T(8,128)(2,1)} %param.27) | copy-start | bytes 12582916
  97.0 71.8 %copy-start.11 = (bf16[1,4096,512]{2,1,0:T(8,128)(2,1)S(1)}, bf16[1,4096,512]{2,1,0:T(8,128)(2,1)}, u32[]{:S(2)}) copy-start(bf16[1,4096,512]{2,1,0:T(8,128)(2,1)} %param.25) | copy-start | bytes 12582916
  97.0 71.8 %copy-start.12 = (bf16[1,4096,512]{2,1,0:T(8,128)(2,1)S(1)}, bf16[1,4096,512]{2,1,0:T(8,128)(2,1)}, u32[]{:S(2)}) copy-start(bf16[1,4096,512]{2,1,0:T(8,128)(2,1)} %param.26) | copy-start | bytes 12582916
